TPU v7x, 256 devices: a whole 4x4x8 slice. The times are simulated.
256 devices in a mesh: kv: 64 (over z, y, core), tp: 4 (over x).
Axes of the slice: x: 4, y: 4, z: 8, core: 2. Of those that a mesh axis runs over, the one named last changes fastest.
Arguments:
- hidden_vectors: bfloat16 [512, 2048], P(None, 'kv'), may hold values from -24 to 24
- input_norm_gain: float32 [2048], P('kv'), may hold values from 0.1 to 1.9
- gate_matrix: bfloat16 [2048, 4096], P('kv', 'tp'), may hold values from -0.125 to 0.125
- value_matrix: bfloat16 [2048, 4096], P('kv', 'tp'), may hold values from -0.125 to 0.125
- write_matrix: bfloat16 [2048, 2048], P('kv', 'tp'), may hold values from -0.125 to 0.125
- read_matrix: bfloat16 [2048, 2048], P('kv', 'tp'), may hold values from -0.125 to 0.125
- step_matrix: bfloat16 [2048, 64], P('kv', 'tp'), may hold values from -0.125 to 0.125
- raw_value_rows: bfloat16 [128, 7, 4096], P('kv', None, 'tp'), may hold values from -6 to 6
- raw_write_rows: bfloat16 [128, 7, 2048], P('kv', None, 'tp'), may hold values from -6 to 6
- raw_read_rows: bfloat16 [128, 7, 2048], P('kv', None, 'tp'), may hold values from -6 to 6
- value_filter_taps: bfloat16 [4, 4096], P(None, 'tp'), may hold values from -3 to 3
- write_filter_taps: bfloat16 [4, 2048], P(None, 'tp'), may hold values from -3 to 3
- read_filter_taps: bfloat16 [4, 2048], P(None, 'tp'), may hold values from -3 to 3
- step_size_bias: float32 [64], P('tp'), may hold values from -3 to 0
- rate_logarithm: float32 [64], P('tp'), may hold values from -4 to 0.5
- direct_path_gain: float32 [64], P('tp'), may hold values from 0.1 to 1.9
- prior_step_preact: float32 [128, 4, 64], P('kv', None, 'tp'), may hold values from -6 to 6
- extra_log_decay: float32 [128, 8, 64], P('kv', None, 'tp'), may hold values from -0.7 to 0, as said below
- accepted: int32 [128], P('kv'), may hold values from 0 to 4
- prior_state: float32 [128, 64, 64, 128], P('kv', 'tp'), may hold values from -6 to 6
- group_norm_gain: float32 [4096], P('tp'), may hold values from 0.1 to 1.9
- output_matrix: bfloat16 [4096, 2048], P('tp', 'kv'), may hold values from -0.09375 to 0.09375
Outputs:
- mixer_out: bfloat16 [512, 2048], P('tp', 'kv')
- resumed_state: float32 [128, 64, 64, 128], P('kv', 'tp')
Inputs may be any that keep to these rules, and one draw needn't show every extreme that they name: `extra_log_decay`: zero at most positions.
All inputs are finite; a program needn't handle non-finite values.
Results may differ from a plain program's by a relative error of at most 0.0095.
Values may be sent and summed in bfloat16 or wider, within the bound.
A program may use at most 64 MiB of HBM per device.

v0:
```python
import jax
import jax.numpy as jnp
from jax import lax
from jax.sharding import Mesh
from jax.sharding import PartitionSpec as P

D = 2048
HEAD_DIM = 64
GROUPS = 16
STATE = 128
TAPS = 4
DRAFT_TOKENS = 4
INNER = 4096
KV = ("kv_0", "kv_1", "kv_2")


epsilon = 1e-06
highest = lax.Precision.HIGHEST


def laid_out(pieces, dim):
    pieces = jnp.moveaxis(pieces, 0, dim)
    lengths = pieces.shape
    return pieces.reshape(*lengths[:dim], lengths[dim] * lengths[dim + 1], *lengths[dim + 2 :])


def all_blocks(value, axes, order):
    pieces = value[None]
    for k in order:
        pieces = lax.all_gather(pieces, axes[k], axis=0, tiled=True)
    current = [lax.axis_size(axes[k]) for k in reversed(order)]
    pieces = pieces.reshape(*current, *value.shape)
    turned = sorted(range(len(order)), key=lambda place: order[len(order) - 1 - place])
    return pieces.transpose(*turned, *range(len(order), pieces.ndim)).reshape(-1, *value.shape)


def whole_of(value, axes, order, dim):
    return laid_out(all_blocks(value, axes, order), dim)


def from_everyone(value, axis):
    copies = jnp.broadcast_to(value, (lax.axis_size(axis), *value.shape))
    return lax.all_to_all(copies, axis, split_axis=0, concat_axis=0, tiled=True)


def of_everyone(value, axis):
    return from_everyone(value, axis).sum(axis=0)


def gather_directly(value, axis, dim):
    return laid_out(from_everyone(value, axis), dim)


def in_blocks(value, dim, devices):
    lengths = value.shape
    pieces = value.reshape(*lengths[:dim], devices, lengths[dim] // devices, *lengths[dim + 1 :])
    return jnp.moveaxis(pieces, dim, 0)


def sum_at_owner(value, axis, dim):
    pieces = in_blocks(value, dim, lax.axis_size(axis))
    arrived = lax.all_to_all(pieces, axis, split_axis=0, concat_axis=0, tiled=True)
    return arrived.astype(jnp.float32).sum(axis=0)


def conv_rows(row_block, taps):
    length_rows = row_block.shape[1] - (TAPS - 1)
    result = jnp.zeros((row_block.shape[0], length_rows, row_block.shape[2]), jnp.float32)
    for tap_index in range(TAPS):
        result = result + row_block[:, tap_index : tap_index + length_rows].astype(
            jnp.float32
        ) * taps[tap_index].astype(jnp.float32)
    return jax.nn.silu(result)


def resume_state(start_state, values, writes, head_step_size, decay_logarithm, accepted):
    live_mask = (jnp.arange(values.shape[1])[None, :] < accepted[:, None]).astype(jnp.float32)
    kept_decay = decay_logarithm * live_mask[:, :, None]
    total_decay = jnp.sum(kept_decay, axis=1)
    tail_decay = total_decay[:, None, :] - jnp.cumsum(kept_decay, axis=1)
    coefficient = live_mask[:, :, None] * jnp.exp(tail_decay) * head_step_size
    added = jnp.einsum("skh,skhp,skhn->shpn", coefficient, values, writes, precision=highest)
    return jnp.exp(total_decay)[:, :, None, None] * start_state + added


def dual_block(
    values, writes, reads, head_step_size, decay_logarithm, direct_path_gain, start_state
):
    cumulative = jnp.cumsum(decay_logarithm, axis=1)
    carried = jnp.exp(cumulative)[..., None] * jnp.einsum(
        "skhn,shpn->skhp", reads, start_state, precision=highest
    )
    order = jnp.arange(cumulative.shape[1])
    causal = order[:, None] >= order[None, :]
    difference = cumulative[:, :, None, :] - cumulative[:, None, :, :]
    decay_weight = jnp.where(causal[None, :, :, None], jnp.exp(jnp.minimum(difference, 0.0)), 0.0)
    inner_terms = jnp.einsum("sthn,suhn->stuh", reads, writes, precision=highest)
    within = jnp.einsum(
        "stuh,suh,suhp->sthp", inner_terms * decay_weight, head_step_size, values, precision=highest
    )
    return carried + within + direct_path_gain[None, None, :, None] * values


def mixer_kernel_body(
    output_gate,
    fresh_values,
    fresh_writes,
    fresh_reads,
    step_preact,
    raw_value_rows,
    raw_write_rows,
    raw_read_rows,
    value_filter_taps,
    write_filter_taps,
    read_filter_taps,
    step_size_bias,
    rate_logarithm,
    direct_path_gain,
    prior_step_preact,
    extra_log_decay,
    accepted,
    prior_state,
    group_norm_gain,
):
    seq_count = raw_value_rows.shape[0]
    head_count = step_preact.shape[2]
    group_count = fresh_writes.shape[2] // STATE
    per_group = head_count // group_count
    window = accepted[:, None] + jnp.arange(TAPS - 1, dtype=jnp.int32)[None, :]

    def current(row_block, new_rows, taps):
        earlier = jnp.take_along_axis(row_block, window[:, :, None], axis=1)
        return conv_rows(jnp.concatenate([earlier, new_rows], axis=1), taps)

    conv_values = current(raw_value_rows, fresh_values, value_filter_taps).reshape(
        seq_count, DRAFT_TOKENS, head_count, HEAD_DIM
    )
    conv_writes = current(raw_write_rows, fresh_writes, write_filter_taps).reshape(
        seq_count, DRAFT_TOKENS, group_count, STATE
    )
    conv_reads = current(raw_read_rows, fresh_reads, read_filter_taps).reshape(
        seq_count, DRAFT_TOKENS, group_count, STATE
    )
    last_values = conv_rows(raw_value_rows, value_filter_taps).reshape(
        seq_count, DRAFT_TOKENS, head_count, HEAD_DIM
    )
    last_writes = conv_rows(raw_write_rows, write_filter_taps).reshape(
        seq_count, DRAFT_TOKENS, group_count, STATE
    )
    head_decay_rate = jnp.exp(rate_logarithm)
    head_step_size = jax.nn.softplus(step_preact + step_size_bias)
    decay_logarithm = -head_decay_rate * head_step_size + extra_log_decay[:, DRAFT_TOKENS:]
    prior_step = jax.nn.softplus(prior_step_preact + step_size_bias)
    prior_decay = -head_decay_rate * prior_step + extra_log_decay[:, :DRAFT_TOKENS]
    restored_state = resume_state(
        prior_state,
        last_values,
        jnp.repeat(last_writes, per_group, axis=2),
        prior_step,
        prior_decay,
        accepted,
    )
    mixed_heads = dual_block(
        conv_values,
        jnp.repeat(conv_writes, per_group, axis=2),
        jnp.repeat(conv_reads, per_group, axis=2),
        head_step_size,
        decay_logarithm,
        direct_path_gain,
        restored_state,
    )
    gated = mixed_heads.reshape(seq_count, DRAFT_TOKENS, -1) * jax.nn.silu(
        output_gate.astype(jnp.float32)
    )
    group_width = INNER // GROUPS
    grouped = gated.reshape(seq_count, DRAFT_TOKENS, -1, group_width)
    scale = lax.rsqrt(jnp.mean(grouped * grouped, axis=-1, keepdims=True) + epsilon)
    normalized_hidden = (grouped * scale).reshape(seq_count, DRAFT_TOKENS, -1) * group_norm_gain
    return (
        normalized_hidden.astype(jnp.bfloat16).reshape(seq_count * DRAFT_TOKENS, -1),
        restored_state,
    )


def per_device(
    hidden_vectors,
    input_norm_gain,
    gate_matrix,
    value_matrix,
    write_matrix,
    read_matrix,
    step_matrix,
    raw_value_rows,
    raw_write_rows,
    raw_read_rows,
    value_filter_taps,
    write_filter_taps,
    read_filter_taps,
    step_size_bias,
    rate_logarithm,
    direct_path_gain,
    prior_step_preact,
    extra_log_decay,
    accepted,
    prior_state,
    group_norm_gain,
    output_matrix,
):
    floats_in = hidden_vectors.astype(jnp.float32)
    square_part = jnp.sum(floats_in * floats_in, axis=1)
    scaled = (floats_in * input_norm_gain).astype(jnp.bfloat16)
    seq_count = raw_value_rows.shape[0]
    own_rows = seq_count * DRAFT_TOKENS
    role_weights = (gate_matrix, value_matrix, write_matrix, read_matrix)
    widths = tuple((weight.shape[1] for weight in role_weights))
    kv_count = lax.axis_size(KV)
    full_scaled = whole_of(scaled, KV, (1, 0, 2), 1)
    square_total = of_everyone(square_part, KV)
    inverse_all = lax.rsqrt(square_total / D + epsilon)[:, None]
    pieces = [weight.reshape(weight.shape[0], kv_count, -1) for weight in role_weights]
    joined = jnp.concatenate(pieces, axis=2)
    column_block = lax.all_to_all(joined, KV, split_axis=1, concat_axis=0, tiled=True)
    column_block = column_block.reshape(column_block.shape[0], -1)
    step_full = gather_directly(step_matrix, KV, 0)
    local_cols = (
        inverse_all * jnp.dot(full_scaled, column_block, preferred_element_type=jnp.float32)
    ).astype(jnp.bfloat16)
    arrived = lax.all_to_all(local_cols, KV, split_axis=0, concat_axis=1, tiled=True)
    arrived = arrived.reshape(own_rows, kv_count, -1)
    role_parts = []
    lower = 0
    for width in widths:
        piece_width = width // kv_count
        role_parts.append(arrived[:, :, lower : lower + piece_width].reshape(own_rows, width))
        lower = lower + piece_width
    projected = jnp.concatenate(role_parts, axis=1).reshape(seq_count, DRAFT_TOKENS, -1)
    own_start = lax.axis_index(KV) * own_rows
    own_scaled = lax.dynamic_slice_in_dim(full_scaled, own_start, own_rows)
    inverse = lax.dynamic_slice_in_dim(inverse_all, own_start, own_rows)
    step_sum = jnp.dot(own_scaled, step_full, preferred_element_type=jnp.float32)
    first_cut = widths[0]
    second_cut = first_cut + widths[1]
    third_cut = second_cut + widths[2]
    output_gate = projected[:, :, :first_cut]
    fresh_values = projected[:, :, first_cut:second_cut]
    fresh_writes = projected[:, :, second_cut:third_cut]
    fresh_reads = projected[:, :, third_cut:]
    step_preact = (inverse * step_sum).reshape(seq_count, DRAFT_TOKENS, -1)
    normalized_hidden, restored_state = mixer_kernel_body(
        output_gate,
        fresh_values,
        fresh_writes,
        fresh_reads,
        step_preact,
        raw_value_rows,
        raw_write_rows,
        raw_read_rows,
        value_filter_taps,
        write_filter_taps,
        read_filter_taps,
        step_size_bias,
        rate_logarithm,
        direct_path_gain,
        prior_step_preact,
        extra_log_decay,
        accepted,
        prior_state,
        group_norm_gain,
    )
    partial_value = jnp.dot(
        gather_directly(normalized_hidden, KV, 0), output_matrix, preferred_element_type=jnp.float32
    )
    mixer_out = sum_at_owner(partial_value.astype(jnp.bfloat16), "tp", 0).astype(jnp.bfloat16)
    return (mixer_out, restored_state)


def solution(mesh):
    torus = Mesh(mesh.devices.reshape(8, 4, 2, mesh.shape["tp"]), ("kv_0", "kv_1", "kv_2", "tp"))
    return jax.shard_map(
        per_device,
        mesh=torus,
        in_specs=(
            P(None, KV),
            P(KV),
            P(KV, "tp"),
            P(KV, "tp"),
            P(KV, "tp"),
            P(KV, "tp"),
            P(KV, "tp"),
            P(KV, None, "tp"),
            P(KV, None, "tp"),
            P(KV, None, "tp"),
            P(None, "tp"),
            P(None, "tp"),
            P(None, "tp"),
            P("tp"),
            P("tp"),
            P("tp"),
            P(KV, None, "tp"),
            P(KV, None, "tp"),
            P(KV),
            P(KV, "tp", None, None),
            P("tp"),
            P("tp", KV),
        ),
        out_specs=(P("tp", KV), P(KV, "tp", None, None)),
        check_vma=False,
    )
```

profile of v0, /device:TPU:1, one launch (start us, length us, event | category | flops | bytes accessed | tf_op | source)
XLA Modules:
  0.0 177.7 jit_solution(18006357835038504651)
XLA Ops:
  7.3 0.9 fusion.5
  8.2 10.5 %all-gather = bf16[2048,32]{0,1:T(8,128)(2,1)S(1)} all-gather(bf16[512,32]{0,1:T(8,128)(2,1)S(1)} %get-tuple-element.14), channel_id=2, replica_groups=mesh['kv_0'=8,'kv_1'=4,'kv_2'=2,'tp'=4] {'kv_1'}, dimensions={0}, use_global_device_ids=true | all-gather | bytes 163840 | tf_op jit(solution)/shard_map/all_gather | solution.py:30
  18.8 0.7 copy.450
  19.5 0.7 broadcast_bitcast_fusion
  20.2 0.8 reshape.400
  21.0 14.4 %all-to-all-start.1 = ((bf16[64,2,256]{2,1,0:T(2,128)(2,1)}), bf16[64,2,256]{2,1,0:T(2,128)(2,1)S(1)}, u32[]{:S(2)}, u32[]{:S(2)}) async-start(bf16[64,2,256]{2,1,0:T(2,128)(2,1)} %reshape.400), calls=%async_computation.1 | async-start | bytes 131072 | tf_op jit(solution)/shard_map/all_to_all | solution.py:43
  35.5 0.7 and_bitcast_fusion
  36.2 0.7 shift-left_or_fusion
  36.9 0.8 slice_convert_fusion.12
  37.8 0.8 slice_convert_fusion.8
  38.6 21.0 %all-gather.4.cloned.1.call-done = bf16[32,512,32]{1,2,0:T(8,128)(2,1)} async-done(((bf16[4,512,32]{1,2,0:T(8,128)(2,1)}), bf16[32,512,32]{1,2,0:T(8,128)(2,1)}) %all-gather.4.cloned.1.call-update) | async-done | bytes 1048592 | tf_op jit(solution)/shard_map/all_gather | solution.py:30
  60.5 0.6 gather_fusion.1
  61.1 0.6 gather_fusion.2
  61.8 0.6 gather_fusion
  62.7 0.7 broadcast_in_dim.34
  63.4 12.0 %all-to-all-start = ((f32[64,1,512]{2,1,0:T(1,128)}), f32[64,1,512]{2,1,0:T(1,128)S(1)}, u32[]{:S(2)}, u32[]{:S(2)}) async-start(f32[64,1,512]{2,1,0:T(1,128)} %broadcast_in_dim.34), calls=%async_computation | async-start | bytes 262144 | tf_op jit(solution)/shard_map/all_to_all | solution.py:43
  75.9 1.4 reshape.396
  77.3 9.1 %all-to-all-done = f32[64,1,512]{2,1,0:T(1,128)S(1)} async-done(((f32[64,1,512]{2,1,0:T(1,128)}), f32[64,1,512]{2,1,0:T(1,128)S(1)}, u32[]{:S(2)}, u32[]{:S(2)}) %all-to-all-start) | async-done | bytes 131104 | tf_op jit(solution)/shard_map/all_to_all | solution.py:43
  86.5 4.4 %all-to-all-start.2 = ((bf16[64,2,768]{2,1,0:T(2,128)(2,1)}), bf16[64,2,768]{2,1,0:T(2,128)(2,1)S(1)}, u32[]{:S(2)}, u32[]{:S(2)}) async-start(bf16[64,2,768]{2,1,0:T(2,128)(2,1)} %reshape.396), calls=%async_computation.2 | async-start | bytes 393216 | tf_op jit(solution)/shard_map/all_to_all | solution.py:222
  91.7 11.4 %all-to-all-done.2 = bf16[64,2,768]{2,1,0:T(2,128)(2,1)S(1)} async-done(((bf16[64,2,768]{2,1,0:T(2,128)(2,1)}), bf16[64,2,768]{2,1,0:T(2,128)(2,1)S(1)}, u32[]{:S(2)}, u32[]{:S(2)}) %all-to-all-start.2) | async-done | bytes 196640 | tf_op jit(solution)/shard_map/all_to_all | solution.py:222
  103.2 0.5 reshape.397
  103.7 1.7 copy.378
  105.5 0.5 convolution_multiply_fusion.1
  106.2 0.5 fusion
  106.8 0.8 reshape.398
  107.6 4.5 %all-to-all-start.3 = ((bf16[64,2,192]{2,1,0:T(2,128)(2,1)}), bf16[64,2,192]{2,1,0:T(2,128)(2,1)S(1)}, u32[]{:S(2)}, u32[]{:S(2)}) async-start(bf16[64,2,192]{2,1,0:T(2,128)(2,1)} %reshape.398), calls=%async_computation.3 | async-start | bytes 131072 | tf_op jit(solution)/shard_map/all_to_all | solution.py:228
  112.4 9.8 %all-to-all-done.3 = bf16[64,2,192]{2,1,0:T(2,128)(2,1)S(1)} async-done(((bf16[64,2,192]{2,1,0:T(2,128)(2,1)}), bf16[64,2,192]{2,1,0:T(2,128)(2,1)S(1)}, u32[]{:S(2)}, u32[]{:S(2)}) %all-to-all-start.3) | async-done | bytes 49184 | tf_op jit(solution)/shard_map/all_to_all | solution.py:228
  124.3 1.9 %convolution_add_fusion = f32[2,16,64,128]{3,2,1,0:T(8,128)S(1)} fusion(f32[2,4,16,128]{3,1,2,0:T(4,128)S(1)} %bitcast.112, f32[2,16,64,128]{3,2,1,0:T(8,128)S(1)} %copy-done.3, f32[2,16]{1,0:T(2,128)S(1)} %exp.59, f32[2,4,16,64]{3,2,1,0:T(8,128)S(1)} %reshape.339, f32[2,4,16]{1,2,0:T(8,128)S(1)} %copy.380), kind=kOutput, calls=%fused_computation.3 | convolution fusion | flops 13115392 | bytes 2196096 | tf_op jit(solution)/shard_map/skh,skhp,skhn->shpn/dot_general | solution.py:82
  126.3 1.7 fusion.27
  129.7 32.0 %all_to_all.52 = bf16[64,8,1024]{2,1,0:T(8,128)(2,1)S(1)} all-to-all(bf16[64,8,1024]{2,1,0:T(8,128)(2,1)S(1)} %broadcast_in_dim.43), channel_id=1, replica_groups=mesh['kv_0'=8,'kv_1'=4,'kv_2'=2,'tp'=4] {'kv_0','kv_1','kv_2'}, dimensions={0} | all-to-all | bytes 2097152 | tf_op jit(solution)/shard_map/all_to_all | solution.py:43
  162.1 8.1 %all_to_all.53 = bf16[4,128,32]{1,2,0:T(8,128)(2,1)S(1)} all-to-all(bf16[4,128,32]{1,2,0:T(8,128)(2,1)S(1)} %bitcast.114), channel_id=1, replica_groups=mesh['kv_0'=8,'kv_1'=4,'kv_2'=2,'tp'=4] {'tp'}, dimensions={0} | all-to-all | bytes 65536 | tf_op jit(solution)/shard_map/all_to_all | solution.py:62
  170.2 0.6 reduce_sum.61
  (112 shorter events, 7.2 us)
Async XLA Ops:
  7.2 154.5 %copy-start = (bf16[1024,32]{0,1:T(8,128)(2,1)S(1)}, bf16[1024,32]{0,1:T(8,128)(2,1)}, u32[]{:S(2)}) copy-start(bf16[1024,32]{0,1:T(8,128)(2,1)} %param.45) | copy-start | bytes 196612
  7.2 52.5 %copy-start.16 = (s32[2]{0:T(128)S(1)}, s32[2]{0:T(128)}, u32[]{:S(2)}) copy-start(s32[2]{0:T(128)} %param.42) | copy-start | bytes 28
  7.2 52.6 %copy-start.6 = (bf16[32,1024]{1,0:T(8,128)(2,1)S(1)}, bf16[32,1024]{1,0:T(8,128)(2,1)}, u32[]{:S(2)}) copy-start(bf16[32,1024]{1,0:T(8,128)(2,1)} %param.26) | copy-start | bytes 196612
  7.2 52.7 %copy-start.7 = (bf16[32,1024]{1,0:T(8,128)(2,1)S(1)}, bf16[32,1024]{1,0:T(8,128)(2,1)}, u32[]{:S(2)}) copy-start(bf16[32,1024]{1,0:T(8,128)(2,1)} %param.27) | copy-start | bytes 196612
  7.2 52.9 %copy-start.8 = (bf16[32,512]{1,0:T(8,128)(2,1)S(1)}, bf16[32,512]{1,0:T(8,128)(2,1)}, u32[]{:S(2)}) copy-start(bf16[32,512]{1,0:T(8,128)(2,1)} %param.28) | copy-start | bytes 98308
  7.2 53.0 %copy-start.9 = (bf16[32,512]{1,0:T(8,128)(2,1)S(1)}, bf16[32,512]{1,0:T(8,128)(2,1)}, u32[]{:S(2)}) copy-start(bf16[32,512]{1,0:T(8,128)(2,1)} %param.29) | copy-start | bytes 98308
  7.2 53.2 %copy-start.5 = (bf16[2,7,512]{2,0,1:T(2,128)(2,1)S(1)}, bf16[2,7,512]{2,0,1:T(2,128)(2,1)}, u32[]{:S(2)}) copy-start(bf16[2,7,512]{2,0,1:T(2,128)(2,1)} %param.33) | copy-start | bytes 43012
  7.2 53.9 %copy-start.4 = (bf16[2,7,512]{2,0,1:T(2,128)(2,1)S(1)}, bf16[2,7,512]{2,0,1:T(2,128)(2,1)}, u32[]{:S(2)}) copy-start(bf16[2,7,512]{2,0,1:T(2,128)(2,1)} %param.32) | copy-start | bytes 43012
  7.3 54.5 %copy-start.2 = (bf16[2,7,1024]{2,0,1:T(2,128)(2,1)S(1)}, bf16[2,7,1024]{2,0,1:T(2,128)(2,1)}, u32[]{:S(2)}) copy-start(bf16[2,7,1024]{2,0,1:T(2,128)(2,1)} %param.31) | copy-start | bytes 86020
  7.3 55.1 %copy-start.10 = (bf16[4,1024]{1,0:T(4,128)(2,1)S(1)}, bf16[4,1024]{1,0:T(4,128)(2,1)}, u32[]{:S(2)}) copy-start(bf16[4,1024]{1,0:T(4,128)(2,1)} %param.34) | copy-start | bytes 24580
  7.3 52.4 %all-gather.4.cloned.1.call-start = ((), (), s32[]{:S(2)}) async-start(), calls=%async_computation.6 | async-start | bytes 1179648 | tf_op jit(solution)/shard_map/all_gather | solution.py:30
  21.0 41.7 %all-to-all-start.1 = ((bf16[64,2,256]{2,1,0:T(2,128)(2,1)}), bf16[64,2,256]{2,1,0:T(2,128)(2,1)S(1)}, u32[]{:S(2)}, u32[]{:S(2)}) async-start(bf16[64,2,256]{2,1,0:T(2,128)(2,1)} %reshape.400), calls=%async_computation.1 | async-start | bytes 131072 | tf_op jit(solution)/shard_map/all_to_all | solution.py:43
  35.4 68.3 %all-gather.6.cloned.1.call-start = ((), (), s32[]{:S(2)}) async-start(), calls=%async_computation.7 | async-start | bytes 3145728 | tf_op jit(solution)/shard_map/all_gather | solution.py:30
  63.4 23.1 %all-to-all-start = ((f32[64,1,512]{2,1,0:T(1,128)}), f32[64,1,512]{2,1,0:T(1,128)S(1)}, u32[]{:S(2)}, u32[]{:S(2)}) async-start(f32[64,1,512]{2,1,0:T(1,128)} %broadcast_in_dim.34), calls=%async_computation | async-start | bytes 262144 | tf_op jit(solution)/shard_map/all_to_all | solution.py:43
  75.4 15.6 %copy-start.17 = (f32[16]{0:T(128)S(1)}, f32[16]{0:T(128)}, u32[]{:S(2)}) copy-start(f32[16]{0:T(128)} %param.38) | copy-start | bytes 196
  86.5 16.7 %all-to-all-start.2 = ((bf16[64,2,768]{2,1,0:T(2,128)(2,1)}), bf16[64,2,768]{2,1,0:T(2,128)(2,1)S(1)}, u32[]{:S(2)}, u32[]{:S(2)}) async-start(bf16[64,2,768]{2,1,0:T(2,128)(2,1)} %reshape.396), calls=%async_computation.2 | async-start | bytes 393216 | tf_op jit(solution)/shard_map/all_to_all | solution.py:222
  103.7 2.3 %copy-start.11 = (f32[2,4,16]{2,1,0:T(4,128)S(1)}, f32[2,4,16]{2,1,0:T(4,128)}, u32[]{:S(2)}) copy-start(f32[2,4,16]{2,1,0:T(4,128)} %param.40) | copy-start | bytes 1540
  103.7 2.3 %copy-start.12 = (f32[2,8,16]{2,1,0:T(8,128)S(1)}, f32[2,8,16]{2,1,0:T(8,128)}, u32[]{:S(2)}) copy-start(f32[2,8,16]{2,1,0:T(8,128)} %param.41) | copy-start | bytes 3076
  103.7 2.3 %copy-start.14 = (f32[16]{0:T(128)S(1)}, f32[16]{0:T(128)}, u32[]{:S(2)}) copy-start(f32[16]{0:T(128)} %param.37) | copy-start | bytes 196
  106.7 17.5 %copy-start.3 = (f32[2,16,64,128]{3,2,1,0:T(8,128)S(1)}, f32[2,16,64,128]{3,2,1,0:T(8,128)}, u32[]{:S(2)}) copy-start(f32[2,16,64,128]{3,2,1,0:T(8,128)} %param.43) | copy-start | bytes 3145732
  107.6 14.6 %all-to-all-start.3 = ((bf16[64,2,192]{2,1,0:T(2,128)(2,1)}), bf16[64,2,192]{2,1,0:T(2,128)(2,1)S(1)}, u32[]{:S(2)}, u32[]{:S(2)}) async-start(bf16[64,2,192]{2,1,0:T(2,128)(2,1)} %reshape.398), calls=%async_computation.3 | async-start | bytes 131072 | tf_op jit(solution)/shard_map/all_to_all | solution.py:228
  124.2 4.7 %copy-start.15 = (f32[16]{0:T(128)S(1)}, f32[16]{0:T(128)}, u32[]{:S(2)}) copy-start(f32[16]{0:T(128)} %param.39) | copy-start | bytes 196
  124.3 5.3 %copy-start.13 = (f32[1024]{0:T(1024)S(1)}, f32[1024]{0:T(1024)}, u32[]{:S(2)}) copy-start(f32[1024]{0:T(1024)} %param.44) | copy-start | bytes 12292
  126.2 35.5 %copy-start.1 = (f32[2,16,64,128]{3,2,1,0:T(8,128)}, f32[2,16,64,128]{3,2,1,0:T(8,128)S(1)}, u32[]{:S(2)}) copy-start(f32[2,16,64,128]{3,2,1,0:T(8,128)S(1)} %convolution_add_fusion) | copy-start | bytes 3145732
Sparse Core Ops, SparseCore 0:
  19.6 40.0 all-gather.3
  61.4 19.2 all-gather.5
where the time goes:
time: 179 us; the launch traced here: 178 us
  waiting for transfers between devices  51.5 us (29%)
  blocking collectives  50.6 us (28%)
  starting transfers between devices  35.3 us (20%)
  between operations  14.6 us (8%)
  local copies, waits for them, and re-layouts  13.6 us (8%)
  other arithmetic  6.1 us (3%)
  matrix products  5.87 us (3%)
    all_to_all x1, blocking collectives, from_everyone(): return lax.all_to_all(copies, axis, split_axis=0, concat_axis=0, tiled=True)  32 us
    all_to_all x2, starting transfers between devices, from_everyone(): return lax.all_to_all(copies, axis, split_axis=0, concat_axis=0, tiled=True)  26.4 us
    all_gather x2, waiting for transfers between devices, all_blocks(): pieces = lax.all_gather(pieces, axes[k], axis=0, tiled=True)  21.1 us
    all_to_all x1, waiting for transfers between devices, per_device(): lax.all_to_all(joined, KV, split_axis=1, concat_axis=0, tiled=True)  11.4 us
    all_gather x1, blocking collectives, all_blocks(): pieces = lax.all_gather(pieces, axes[k], axis=0, tiled=True)  10.5 us
    all_to_all x1, waiting for transfers between devices, per_device(): lax.all_to_all(local_cols, KV, split_axis=0, concat_axis=1, tiled=True)  9.8 us
    all_to_all x2, waiting for transfers between devices, from_everyone(): return lax.all_to_all(copies, axis, split_axis=0, concat_axis=0, tiled=True)  9.15 us
    all_to_all x1, blocking collectives, sum_at_owner(): lax.all_to_all(pieces, axis, split_axis=0, concat_axis=0, tiled=True)  8.15 us
  transfers between devices with their start and end apart: 6, of which 4 were waited for; matrix products, arithmetic and copies ran while one was open for 7% of the time, Pallas kernels for 0%

commit v1 on v0

v1 whole, which is shorter than its diff:
```python
import jax
import jax.numpy as jnp
from jax import lax
from jax.experimental import pallas as pl
from jax.experimental.pallas import tpu as pltpu
from jax.sharding import PartitionSpec as P

MESH = pl.DeviceIdType.MESH
F32 = jnp.float32
BF16 = jnp.bfloat16
EPS = 1e-6
Z_ORDER = (4, 3, 5, 2, 6, 1, 7, 0)


def silu(x):
    return x / (1.0 + jnp.exp(-x))


def softplus(x):
    return jnp.maximum(x, 0.0) + jnp.log(1.0 + jnp.exp(-jnp.abs(x)))


def mixer_kernel(
    acc_s,
    hid, gain, wg, wv, ww, wr, ws, rawv, raww, rawr, tv, tw, tr, bias, rate, dgain, ppre, extra, prior, ngain, wo,
    out_ref, st_out,
    hid_v, gain_v, wg_v, wv_v, ww_v, wr_v, ws_v, rawv_v, raww_v, rawr_v, tv_v, tw_v, tr_v, bias_v, rate_v, dgain_v,
    ppre_v, extra_v, prior_v, ngain_v, wo_v,
    acts_t, wsend, wblk, sblk, acts_f, acts_b, psend, precv, esend, erecv, tot, fsend, frecv, nrm, wog, osend, orecv,
    base, state_b,
    lsem, osem, s1_send, s1_recv, w_send, w_recv, k_send, k_recv, p_send, p_recv, e_send, e_recv, f_send, f_recv,
    n_send, n_recv, g_send, g_recv, o_send, o_recv, ready,
):
    kv = lax.axis_index("kv")
    tp = lax.axis_index("tp")
    z = lax.div(kv, 8)
    c = lax.rem(kv, 8)

    def plane(r):
        return z * 8 + lax.rem(c + r, 8)

    def ring(r):
        return lax.rem(z + r, 8) * 8 + c

    def remote(src, dst, ssem, rsem, kv_to, tp_to):
        return pltpu.make_async_remote_copy(
            src_ref=src, dst_ref=dst, send_sem=ssem, recv_sem=rsem,
            device_id={"kv": kv_to, "tp": tp_to}, device_id_type=MESH,
        )

    pairs = [
        (hid, hid_v), (gain, gain_v), (wg, wg_v), (wv, wv_v), (ww, ww_v), (wr, wr_v), (ws, ws_v), (wo, wo_v),
        (rawv, rawv_v), (raww, raww_v), (rawr, rawr_v), (tv, tv_v), (tw, tw_v), (tr, tr_v), (bias, bias_v),
        (rate, rate_v), (dgain, dgain_v), (ppre, ppre_v), (extra, extra_v), (ngain, ngain_v), (prior, prior_v),
    ]
    loads = [pltpu.make_async_copy(s, d, lsem.at[i]) for i, (s, d) in enumerate(pairs)]
    for cp in loads:
        cp.start()

    barrier = pltpu.get_barrier_semaphore()
    for r in range(1, 8):
        pl.semaphore_signal(barrier, inc=1, device_id={"kv": plane(r), "tp": tp}, device_id_type=MESH)
    for r in range(1, 8):
        pl.semaphore_signal(barrier, inc=1, device_id={"kv": ring(r), "tp": tp}, device_id_type=MESH)
    for r in range(1, 4):
        pl.semaphore_signal(barrier, inc=1, device_id={"kv": kv, "tp": lax.rem(tp + r, 4)}, device_id_type=MESH)

    own32 = pl.ds(pl.multiple_of(c * 32, 32), 32)
    loads[0].wait()
    acts_t[own32, :] = jnp.transpose(hid_v[...].astype(F32)).astype(BF16)
    for i in range(1, 7):
        loads[i].wait()
    diag = lax.broadcasted_iota(jnp.int32, (32, 32), 0) == lax.broadcasted_iota(jnp.int32, (32, 32), 1)
    gcol = jnp.sum(jnp.where(diag, jnp.broadcast_to(gain_v[...], (32, 32)), 0.0), axis=1, keepdims=True)
    for j in range(8):
        lane = slice(j * 128, j * 128 + 128)
        wsend[j, :, 0:128] = (wg_v[:, lane].astype(F32) * gcol).astype(BF16)
        wsend[j, :, 128:256] = (wv_v[:, lane].astype(F32) * gcol).astype(BF16)
        half = slice((j % 4) * 128, (j % 4) * 128 + 128)
        source = ww_v if j < 4 else wr_v
        wsend[j, :, 256:384] = (source[:, half].astype(F32) * gcol).astype(BF16)
    wblk[own32, :] = wsend[c]
    step_w = (ws_v[...].astype(F32) * gcol).astype(BF16)
    sblk[own32, :] = jnp.concatenate([step_w.astype(F32), jnp.zeros((32, 112), F32)], axis=1).astype(BF16)

    pl.semaphore_wait(barrier, 17)
    for r in range(1, 4):
        pl.semaphore_signal(ready, inc=1, device_id={"kv": kv, "tp": lax.rem(tp + r, 4)}, device_id_type=MESH)

    acts_cp, w_cp, k_cp = [], [], []
    for r in range(1, 8):
        cp = remote(acts_t.at[own32, :], acts_t.at[own32, :], s1_send.at[r], s1_recv.at[r], plane(r), tp)
        cp.start()
        acts_cp.append(cp)
    for r in range(1, 8):
        cp = remote(wsend.at[lax.rem(c + r, 8)], wblk.at[own32, :], w_send.at[r], w_recv.at[r], plane(r), tp)
        cp.start()
        w_cp.append(cp)
        cp = remote(sblk.at[own32, :], sblk.at[own32, :], k_send.at[r], k_recv.at[r], plane(r), tp)
        cp.start()
        k_cp.append(cp)

    loads[7].wait()
    for i in range(8):
        wog[z, :, i * 128:(i + 1) * 128] = jnp.transpose(
            wo_v[i * 128:(i + 1) * 128, :].astype(F32)
        ).astype(BF16)
    g_cp = {}
    for r in range(1, 8):
        g_cp[r] = remote(wog.at[z], wog.at[z], g_send.at[r], g_recv.at[r], ring(r), tp)
    for r in (2, 6, 1, 7):
        g_cp[r].start()

    for cp in loads[8:]:
        cp.wait()
    row8 = lax.broadcasted_iota(jnp.int32, (8, 1), 0)
    tok = lax.rem(row8, 4)

    def down(x, d):
        if d == 0:
            return x
        return jnp.where(tok >= d, pltpu.roll(x, d, axis=0), 0.0)

    def up(x, d):
        return jnp.where(tok + d < 4, pltpu.roll(x, 8 - d, axis=0), 0.0)

    def last_conv(raw, taps):
        parts = []
        for s in range(2):
            rows = raw[s].astype(F32)
            t = taps[...].astype(F32)
            total = rows[0:4] * t[0:1]
            for j in range(1, 4):
                total = total + rows[j:j + 4] * t[j:j + 1]
            parts.append(total)
        return silu(jnp.concatenate(parts, axis=0))

    def base_conv(raw, taps, lo, hi):
        t = taps[...].astype(F32)
        zero = jnp.zeros((1, hi - lo), F32)
        rows_out = []
        for s in range(2):
            rows = raw[s].astype(F32)
            a = acc_s[s]
            win = rows[4:7]
            for k in range(3, -1, -1):
                win = jnp.where(a == k, rows[k:k + 3], win)
            w0, w1, w2 = win[0:1], win[1:2], win[2:3]
            rows_out += [w0 * t[0:1] + w1 * t[1:2] + w2 * t[2:3], w1 * t[0:1] + w2 * t[1:2], w2 * t[0:1], zero]
        base[:, lo:hi] = jnp.concatenate(rows_out, axis=0)

    lastv = last_conv(rawv_v, tv_v)
    lastw = last_conv(raww_v, tw_v)
    base_conv(rawv_v, tv_v, 0, 1024)
    base_conv(raww_v, tw_v, 1024, 1536)
    base_conv(rawr_v, tr_v, 1536, 2048)

    rate_e = -jnp.exp(rate_v[...])
    bias_r = bias_v[...]
    pstep = softplus(jnp.concatenate([ppre_v[0], ppre_v[1]], axis=0) + bias_r)
    pextra = jnp.concatenate([extra_v[0, 0:4], extra_v[1, 0:4]], axis=0)
    nextra = jnp.concatenate([extra_v[0, 4:8], extra_v[1, 4:8]], axis=0)
    limit = jnp.where(row8 < 4, acc_s[0], acc_s[1])
    live = jnp.where(tok < limit, 1.0, 0.0)
    kept = (rate_e * pstep + pextra) * live
    tail = up(kept, 1) + up(kept, 2) + up(kept, 3)
    coef = live * jnp.exp(tail) * pstep
    etot = jnp.exp(kept + tail)
    lane128 = lax.broadcasted_iota(jnp.int32, (8, 128), 1)
    low_half = lane128 < 64

    def spread(e, i):
        a = jnp.broadcast_to(e[:, 2 * i:2 * i + 1], (8, 128))
        b = jnp.broadcast_to(e[:, 2 * i + 1:2 * i + 2], (8, 128))
        return jnp.where(low_half, a, b)

    for g in range(4):
        vals = [lastv[:, (2 * g + i) * 128:(2 * g + i + 1) * 128] * spread(coef, 2 * g + i) for i in range(2)]
        weighted = jnp.concatenate(vals, axis=1)
        lw = lastw[:, g * 128:(g + 1) * 128]
        for s in range(2):
            own_seq = (row8 < 4) if s == 0 else (row8 >= 4)
            added = lax.dot_general(
                weighted, jnp.where(own_seq, lw, 0.0), (((0,), (0,)), ((), ())),
                precision=lax.Precision.HIGHEST, preferred_element_type=F32,
            )
            for i in range(4):
                h = g * 4 + i
                rows = slice(i * 64, i * 64 + 64)
                factor = jnp.broadcast_to(etot[s * 4:s * 4 + 1, h:h + 1], (64, 128))
                new = factor * prior_v[s, g, rows, :] + added[rows, :]
                prior_v[s, g, rows, :] = new
                state_b[s, g, rows, :] = new.astype(BF16)
    state_cp = pltpu.make_async_copy(prior_v, st_out, osem)
    state_cp.start()

    for cp in acts_cp:
        cp.wait_recv()
    for i in range(4):
        block = jnp.transpose(acts_t[:, i * 128:(i + 1) * 128].astype(F32))
        acts_f[i * 128:(i + 1) * 128, :] = block
        acts_b[i * 128:(i + 1) * 128, :] = block.astype(BF16)
    for cp in w_cp:
        cp.wait_recv()
    for cp in k_cp:
        cp.wait_recv()
    p_cp, e_cp = [], []
    for r in Z_ORDER:
        zz = lax.rem(z + r, 8)
        part = jnp.dot(
            acts_b[pl.ds(pl.multiple_of(zz * 64, 64), 64), :], wblk[...], preferred_element_type=F32
        ).astype(BF16)
        xs = acts_f[pl.ds(pl.multiple_of(zz * 64 + c * 8, 8), 8), :]
        ext = jnp.dot(xs.astype(BF16), sblk[...], preferred_element_type=F32)
        ext = jnp.where(lane128 == 16, jnp.sum(xs * xs, axis=1, keepdims=True), ext)
        if r == 0:
            precv[z] = part
            erecv[z] = ext
        else:
            psend[r] = part
            esend[r] = ext
            cp = remote(psend.at[r], precv.at[z], p_send.at[r], p_recv.at[r], ring(r), tp)
            cp.start()
            p_cp.append(cp)
            cp = remote(esend.at[r], erecv.at[z], e_send.at[r], e_recv.at[r], ring(r), tp)
            cp.start()
            e_cp.append(cp)
    for r in (4, 3, 5):
        g_cp[r].start()

    for cp in e_cp:
        cp.wait_recv()
    esum = erecv[0]
    for k in range(1, 8):
        esum = esum + erecv[k]
    inverse = lax.rsqrt(esum[:, 16:17] / 2048.0 + EPS)
    step = softplus(inverse * esum[:, 0:16] + bias_r)
    decay = rate_e * step + nextra
    cum = decay + down(decay, 1) + down(decay, 2) + down(decay, 3)
    pair_w = []
    for d in range(4):
        w = jnp.exp(jnp.minimum(cum - down(cum, d), 0.0)) * down(step, d)
        pair_w.append(jnp.where(tok >= d, w, 0.0))
    ecum = jnp.exp(cum)

    for cp in p_cp:
        cp.wait_recv()
    total = precv[0].astype(F32)
    for k in range(1, 8):
        total = total + precv[k].astype(F32)
    for j in range(8):
        rows = total[j * 8:j * 8 + 8, :]
        two = jnp.concatenate(
            [rows[:, 0:256], jnp.concatenate([rows[:, 256:384], rows[:, 256:384]], axis=1)], axis=0
        )
        fsend[j] = two.astype(BF16)
    frecv[c] = fsend[c]
    f_cp = []
    for r in range(1, 8):
        cp = remote(fsend.at[lax.rem(c + r, 8)], frecv.at[c], f_send.at[r], f_recv.at[r], plane(r), tp)
        cp.start()
        f_cp.append(cp)

    dg = jnp.broadcast_to(dgain_v[...], (8, 16))
    for cp in f_cp:
        cp.wait_recv()

    def fresh(j):
        return frecv[j].astype(F32)

    def rounded(x):
        return (x * inverse).astype(BF16).astype(F32)

    def conv(x, lo, taps, at):
        t = taps[:, at:at + 128].astype(F32)
        y = base[:, lo:lo + 128] + x * t[3:4]
        for d in range(1, 4):
            y = y + down(x, d) * t[3 - d:4 - d]
        return silu(y)

    writes, reads = [], []
    for g in range(4):
        writes.append(conv(rounded(fresh(g)[8:16, 0:128]), 1024 + g * 128, tw_v, g * 128))
        reads.append(conv(rounded(fresh(4 + g)[8:16, 0:128]), 1536 + g * 128, tr_v, g * 128))
    carried = []
    for g in range(4):
        rb = reads[g].astype(BF16)
        both = [
            lax.dot_general(rb, state_b[s, g], (((1,), (1,)), ((), ())), preferred_element_type=F32)
            for s in range(2)
        ]
        carried.append(jnp.where(row8 < 4, both[0], both[1]))
    normed = []
    for g in range(4):
        inner = [jnp.sum(reads[g] * down(writes[g], d), axis=1, keepdims=True) for d in range(4)]
        gated = []
        for i in range(2):
            j = 2 * g + i
            f = fresh(j)
            value = conv(rounded(f[0:8, 128:256]), j * 128, tv_v, j * 128)
            mixed = spread(ecum, j) * carried[g][:, i * 128:(i + 1) * 128] + spread(dg, j) * value
            for d in range(4):
                mixed = mixed + (inner[d] * spread(pair_w[d], j)) * down(value, d)
            gated.append(mixed * silu(rounded(f[0:8, 0:128])))
        mean = (jnp.sum(gated[0] * gated[0], axis=1, keepdims=True)
                + jnp.sum(gated[1] * gated[1], axis=1, keepdims=True)) / 256.0
        scale = lax.rsqrt(mean + EPS)
        for i in range(2):
            j = 2 * g + i
            normed.append(gated[i] * scale * ngain_v[:, j * 128:(j + 1) * 128])
    nrm[c] = jnp.concatenate(
        [jnp.concatenate(normed[0:4], axis=1), jnp.concatenate(normed[4:8], axis=1)], axis=0
    ).astype(BF16)

    n_cp = []
    for r in range(1, 8):
        cp = remote(nrm.at[c], nrm.at[c], n_send.at[r], n_recv.at[r], plane(r), tp)
        cp.start()
        n_cp.append(cp)
    for r in range(1, 8):
        g_cp[r].wait_recv()
    pl.semaphore_wait(ready, 3)
    for cp in n_cp:
        cp.wait_recv()

    nall = nrm[...].reshape(128, 512)
    wall = wog[...].reshape(256, 1024)
    turned = (((1,), (1,)), ((), ()))
    p0 = lax.dot_general(wall[:, 0:512], nall, turned, preferred_element_type=F32)
    p1 = lax.dot_general(wall[:, 512:1024], nall, turned, preferred_element_type=F32)
    both = (p0 + pltpu.roll(p1, 120, axis=1)).astype(BF16)
    osend[...] = both.reshape(8, 32, 128)

    owner = lax.div(z, 2)
    slot = tp * 2 + lax.rem(z, 2)
    o_cp = []
    for r in (4, 3, 5, 2, 6, 1, 7):
        cp = remote(osend.at[lax.rem(z + r, 8)], orecv.at[slot], o_send.at[r], o_recv.at[slot], ring(r), owner)
        cp.start()
        o_cp.append(cp)
    straight = remote(osend.at[z], orecv.at[slot], o_send.at[0], o_recv.at[slot], kv, owner)

    @pl.when(owner != tp)
    def _():
        straight.start()

    @pl.when(owner == tp)
    def _():
        orecv[slot] = osend[z]

    for i in range(8):
        mine = jnp.logical_and(tp == i // 2, z == tp * 2 + i % 2)

        @pl.when(jnp.logical_not(mine))
        def _():
            remote(osend.at[0], orecv.at[i], o_send.at[1], o_recv.at[i], kv, tp).wait_recv()

    sums = []
    for q in range(2):
        s4 = orecv[q].astype(F32)
        for x in range(1, 4):
            s4 = s4 + orecv[x * 2 + q].astype(F32)
        sums.append(s4)
    lane32 = lax.broadcasted_iota(jnp.int32, (32, 128), 1)
    merged = jnp.transpose(jnp.where(lax.rem(lane32, 16) < 8, sums[0], pltpu.roll(sums[1], 8, axis=1)))
    ordered = [merged[j * 16 + q * 8:j * 16 + q * 8 + 8, :] for q in range(2) for j in range(8)]
    out_ref[...] = jnp.concatenate(ordered, axis=0).astype(BF16)

    state_cp.wait()
    for cp in acts_cp + w_cp + k_cp + p_cp + e_cp + f_cp + n_cp + o_cp + [g_cp[r] for r in range(1, 8)]:
        cp.wait_send()

    @pl.when(owner != tp)
    def _():
        straight.wait_send()


def per_device(
    hidden_vectors, input_norm_gain, gate_matrix, value_matrix, write_matrix, read_matrix, step_matrix,
    raw_value_rows, raw_write_rows, raw_read_rows, value_filter_taps, write_filter_taps, read_filter_taps,
    step_size_bias, rate_logarithm, direct_path_gain, prior_step_preact, extra_log_decay, accepted, prior_state,
    group_norm_gain, output_matrix,
):
    operands = [
        hidden_vectors, input_norm_gain.reshape(1, 32), gate_matrix, value_matrix, write_matrix, read_matrix,
        step_matrix, raw_value_rows, raw_write_rows, raw_read_rows, value_filter_taps, write_filter_taps,
        read_filter_taps, step_size_bias.reshape(1, 16), rate_logarithm.reshape(1, 16),
        direct_path_gain.reshape(1, 16), prior_step_preact, extra_log_decay, prior_state.reshape(2, 4, 256, 128),
        group_norm_gain.reshape(1, 1024), output_matrix,
    ]
    buffers = [pltpu.VMEM(x.shape, x.dtype) for x in operands]
    dma = pltpu.SemaphoreType.DMA
    scratch = buffers + [
        pltpu.VMEM((256, 512), BF16),
        pltpu.VMEM((8, 32, 384), BF16),
        pltpu.VMEM((256, 384), BF16),
        pltpu.VMEM((256, 128), BF16),
        pltpu.VMEM((512, 256), F32),
        pltpu.VMEM((512, 256), BF16),
        pltpu.VMEM((8, 64, 384), BF16),
        pltpu.VMEM((8, 64, 384), BF16),
        pltpu.VMEM((8, 8, 128), F32),
        pltpu.VMEM((8, 8, 128), F32),
        pltpu.VMEM((64, 384), F32),
        pltpu.VMEM((8, 16, 256), BF16),
        pltpu.VMEM((8, 16, 256), BF16),
        pltpu.VMEM((8, 16, 512), BF16),
        pltpu.VMEM((8, 32, 1024), BF16),
        pltpu.VMEM((8, 32, 128), BF16),
        pltpu.VMEM((8, 32, 128), BF16),
        pltpu.VMEM((8, 2048), F32),
        pltpu.VMEM((2, 4, 256, 128), BF16),
        dma((len(operands),)),
        dma,
    ] + [dma((8,)) for _ in range(18)] + [pltpu.SemaphoreType.REGULAR]
    out, state = pl.pallas_call(
        mixer_kernel,
        out_shape=(
            jax.ShapeDtypeStruct((128, 32), BF16),
            jax.ShapeDtypeStruct((2, 4, 256, 128), F32),
        ),
        in_specs=[pl.BlockSpec(memory_space=pltpu.SMEM)] + [pl.BlockSpec(memory_space=pl.ANY)] * len(operands),
        out_specs=(pl.BlockSpec(memory_space=pltpu.VMEM), pl.BlockSpec(memory_space=pl.ANY)),
        scratch_shapes=scratch,
        compiler_params=pltpu.CompilerParams(
            collective_id=0, has_side_effects=True, vmem_limit_bytes=32 * 1024 * 1024
        ),
        cost_estimate=pl.CostEstimate(flops=10**9, bytes_accessed=4 * 10**6, transcendentals=10**5),
        name="mixer",
    )(accepted, *operands)
    return out, state.reshape(2, 16, 64, 128)


def solution(mesh):
    return jax.shard_map(
        per_device,
        mesh=mesh,
        in_specs=(
            P(None, "kv"),
            P("kv"),
            P("kv", "tp"),
            P("kv", "tp"),
            P("kv", "tp"),
            P("kv", "tp"),
            P("kv", "tp"),
            P("kv", None, "tp"),
            P("kv", None, "tp"),
            P("kv", None, "tp"),
            P(None, "tp"),
            P(None, "tp"),
            P(None, "tp"),
            P("tp"),
            P("tp"),
            P("tp"),
            P("kv", None, "tp"),
            P("kv", None, "tp"),
            P("kv"),
            P("kv", "tp", None, None),
            P("tp"),
            P("tp", "kv"),
        ),
        out_specs=(P("tp", "kv"), P("kv", "tp", None, None)),
        check_vma=False,
    )
```

time: 179 us -> 57.1 us (0.32)
  waiting for transfers between devices: 51.5 us -> 0 us
  blocking collectives: 50.6 us -> 0 us
  Pallas kernels: 0 us -> 49.1 us
  starting transfers between devices: 35.3 us -> 0 us
  between operations: 14.6 us -> 0.87 us
  local copies, waits for them, and re-layouts: 13.6 us -> 6.78 us
  other arithmetic: 6.1 us -> 0 us
  matrix products: 5.87 us -> 0 us
    pallas_call x0 -> x1, Pallas kernels: none -> 49.1 us  [per_device(): pl.pallas_call(mixer_kernel, out_shape=(jax.ShapeDtypeStruct((128, 32), B...]
    all_to_all x2 -> x0, blocking collectives: 40.1 us -> none  [the longest x1 32 us: from_everyone(): return lax.all_to_all(copies, axis, split_axis=0, concat_axis=0, tiled=True)]
    all_to_all x4 -> x0, starting transfers between devices: 35.3 us -> none  [the longest x2 26.4 us: from_everyone(): return lax.all_to_all(copies, axis, split_axis=0, concat_axis=0, tiled=True)]
    all_to_all x4 -> x0, waiting for transfers between devices: 30.4 us -> none  [the longest x1 11.4 us: per_device(): lax.all_to_all(joined, KV, split_axis=1, concat_axis=0, tiled=True)]
    all_gather x2 -> x0, waiting for transfers between devices: 21.1 us -> none  [all_blocks(): pieces = lax.all_gather(pieces, axes[k], axis=0, tiled=True)]
    all_gather x1 -> x0, blocking collectives: 10.5 us -> none  [all_blocks(): pieces = lax.all_gather(pieces, axes[k], axis=0, tiled=True)]
    dot_general x7 -> x0, matrix products: 5.87 us -> none  [the longest x1 1.92 us: resume_state(): jnp.einsum('skh,skhp,skhn->shpn', coefficient, values, writes, precision=...]
    gather x7 -> x0, local copies, waits for them, and re-layouts: 1.99 us -> none  [current(): earlier = jnp.take_along_axis(row_block, window[:, :, None], axis=1)]
  transfers between devices with their start and end apart: 6 -> 0, of which waited for: 4 -> 0; matrix products, arithmetic and copies ran while one was open for 7% -> 0% of each run, Pallas kernels for 0% -> 0%
where the time goes in v1:
time: 57.1 us; the launch traced here: 56.7 us
  Pallas kernels  49.1 us (86%)
  local copies, waits for them, and re-layouts  6.78 us (12%)
  between operations  0.87 us (2%)
    pallas_call x1, Pallas kernels, per_device(): pl.pallas_call(mixer_kernel, out_shape=(jax.ShapeDtypeStruct((128, 32), B...  49.1 us
    unnamed x50, local copies, waits for them, and re-layouts  6.78 us

profile of v1, /device:TPU:1, one launch (start us, length us, event | category | flops | bytes accessed | tf_op | source)
XLA Modules:
  0.0 56.7 jit_solution(6339649180529963734)
XLA Ops:
  0.6 0.0 copy-start.19
  0.6 0.0 copy-start.20
  0.7 0.8 %copy.25.ws = bf16[32,16]{1,0:T(8,128)(2,1)S(1)} copy(bf16[32,16]{0,1:T(8,128)(2,1)} %param.28) | data formatting | bytes 2048 | tf_op args[6]
  1.4 0.0 copy-done.19
  1.4 0.0 copy-done.20
  1.5 0.7 %copy-done.18 = bf16[2,7,1024]{2,0,1:T(2,128)(2,1)S(1)} copy-done((bf16[2,7,1024]{2,0,1:T(2,128)(2,1)S(1)}, bf16[2,7,1024]{2,0,1:T(2,128)(2,1)}, u32[]{:S(2)}) %copy-start.18) | copy-done | bytes 28696
  2.2 0.7 %copy-done.17 = bf16[512,32]{0,1:T(8,128)(2,1)S(1)} copy-done((bf16[512,32]{0,1:T(8,128)(2,1)S(1)}, bf16[512,32]{0,1:T(8,128)(2,1)}, u32[]{:S(2)}) %copy-start.17) | copy-done | bytes 32792
  2.9 0.1 copy.24.hid
  3.1 0.7 %copy-done.16 = bf16[1024,32]{0,1:T(8,128)(2,1)S(1)} copy-done((bf16[1024,32]{0,1:T(8,128)(2,1)S(1)}, bf16[1024,32]{0,1:T(8,128)(2,1)}, u32[]{:S(2)}) %copy-start.16) | copy-done | bytes 65560
  3.8 0.0 copy-start.5
  3.8 0.0 copy-start.6
  3.8 0.0 copy-start.7
  3.8 0.0 copy-start.8
  3.8 0.0 copy-start.9
  3.9 0.0 copy-start.10
  3.9 0.0 copy-start.11
  3.9 0.0 copy-start.12
  3.9 0.0 copy-start.13
  3.9 0.0 copy-start.14
  3.9 0.0 copy-start.15
  3.9 0.2 copy.29.wo
  4.1 0.5 copy-done.1
  4.6 0.0 copy-done.2
  4.7 0.0 copy-done.3
  4.7 0.0 copy-done.4
  4.7 0.0 copy-done.5
  4.7 0.0 copy-done.6
  4.8 0.0 copy-start
  4.8 1.2 %copy-done = f32[2,16,64,128]{3,2,1,0:T(8,128)S(1)} copy-done((f32[2,16,64,128]{3,2,1,0:T(8,128)S(1)}, f32[2,16,64,128]{3,2,1,0:T(8,128)}, u32[]{:S(2)}) %copy-start) | copy-done | bytes 1048600
  6.0 49.1 %mixer.1 = (bf16[128,32]{1,0:T(8,128)(2,1)S(1)}, f32[2,4,256,128]{3,2,1,0:T(8,128)S(1)}) custom-call(s32[2]{0:T(128)S(1)} %copy-done.11, bf16[512,32]{1,0:T(8,128)(2,1)S(1)} %copy.24.hid, f32[1,32]{1,0:T(1,128)S(1)} %bitcast.10, bf16[32,1024]{1,0:T(8,128)(2,1)S(1)} %copy-done.1, bf16[32,1024]{1,0:T(8,128)(2,1)S(1)} %copy-done.2, ...), custom_call_target="tpu_custom_call" | custom-call | flops 1000000000 | bytes 4000000 | tf_op jit(solution)/shard_map/mixer/pallas_call | solution.py:416
  55.1 0.7 %copy.30 = bf16[128,32]{0,1:T(8,128)(2,1)} copy(bf16[128,32]{1,0:T(8,128)(2,1)S(1)} %get-tuple-element.6) | data formatting | bytes 16384
  55.7 1.0 %copy.32 = f32[2,16,64,128]{3,2,1,0:T(8,128)} copy(f32[2,16,64,128]{3,2,1,0:T(8,128)S(1)} %bitcast.7) | data formatting | bytes 2097152
  (19 shorter events, 0.0 us)
Async XLA Ops:
  0.6 0.8 %copy-start.19 = (bf16[2,7,512]{2,0,1:T(2,128)(2,1)S(1)}, bf16[2,7,512]{2,0,1:T(2,128)(2,1)}, u32[]{:S(2)}) copy-start(bf16[2,7,512]{2,0,1:T(2,128)(2,1)} %param.30) | copy-start | bytes 43012
  0.6 0.8 %copy-start.20 = (bf16[2,7,512]{2,0,1:T(2,128)(2,1)S(1)}, bf16[2,7,512]{2,0,1:T(2,128)(2,1)}, u32[]{:S(2)}) copy-start(bf16[2,7,512]{2,0,1:T(2,128)(2,1)} %param.31) | copy-start | bytes 43012
  1.4 0.8 %copy-start.18 = (bf16[2,7,1024]{2,0,1:T(2,128)(2,1)S(1)}, bf16[2,7,1024]{2,0,1:T(2,128)(2,1)}, u32[]{:S(2)}) copy-start(bf16[2,7,1024]{2,0,1:T(2,128)(2,1)} %param.29) | copy-start | bytes 86020
  2.2 0.8 %copy-start.17 = (bf16[512,32]{0,1:T(8,128)(2,1)S(1)}, bf16[512,32]{0,1:T(8,128)(2,1)}, u32[]{:S(2)}) copy-start(bf16[512,32]{0,1:T(8,128)(2,1)} %param.22) | copy-start | bytes 98308
  2.9 0.8 %copy-start.16 = (bf16[1024,32]{0,1:T(8,128)(2,1)S(1)}, bf16[1024,32]{0,1:T(8,128)(2,1)}, u32[]{:S(2)}) copy-start(bf16[1024,32]{0,1:T(8,128)(2,1)} %param.43) | copy-start | bytes 196612
  3.8 0.8 %copy-start.1 = (bf16[32,1024]{1,0:T(8,128)(2,1)S(1)}, bf16[32,1024]{1,0:T(8,128)(2,1)}, u32[]{:S(2)}) copy-start(bf16[32,1024]{1,0:T(8,128)(2,1)} %wg.1) | copy-start | bytes 196612
  3.8 0.9 %copy-start.2 = (bf16[32,1024]{1,0:T(8,128)(2,1)S(1)}, bf16[32,1024]{1,0:T(8,128)(2,1)}, u32[]{:S(2)}) copy-start(bf16[32,1024]{1,0:T(8,128)(2,1)} %wv.1) | copy-start | bytes 196612
  3.8 0.9 %copy-start.3 = (bf16[32,512]{1,0:T(8,128)(2,1)S(1)}, bf16[32,512]{1,0:T(8,128)(2,1)}, u32[]{:S(2)}) copy-start(bf16[32,512]{1,0:T(8,128)(2,1)} %ww.1) | copy-start | bytes 98308
  3.8 0.9 %copy-start.4 = (bf16[32,512]{1,0:T(8,128)(2,1)S(1)}, bf16[32,512]{1,0:T(8,128)(2,1)}, u32[]{:S(2)}) copy-start(bf16[32,512]{1,0:T(8,128)(2,1)} %wr.1) | copy-start | bytes 98308
  3.8 0.9 %copy-start.5 = (bf16[4,1024]{1,0:T(4,128)(2,1)S(1)}, bf16[4,1024]{1,0:T(4,128)(2,1)}, u32[]{:S(2)}) copy-start(bf16[4,1024]{1,0:T(4,128)(2,1)} %tv.1) | copy-start | bytes 24580
  3.8 0.9 %copy-start.6 = (f32[2,8,16]{2,1,0:T(8,128)S(1)}, f32[2,8,16]{2,1,0:T(8,128)}, u32[]{:S(2)}) copy-start(f32[2,8,16]{2,1,0:T(8,128)} %extra.1) | copy-start | bytes 3076
  3.8 0.9 %copy-start.7 = (bf16[4,512]{1,0:T(4,128)(2,1)S(1)}, bf16[4,512]{1,0:T(4,128)(2,1)}, u32[]{:S(2)}) copy-start(bf16[4,512]{1,0:T(4,128)(2,1)} %tw.1) | copy-start | bytes 12292
  3.8 0.8 %copy-start.8 = (bf16[4,512]{1,0:T(4,128)(2,1)S(1)}, bf16[4,512]{1,0:T(4,128)(2,1)}, u32[]{:S(2)}) copy-start(bf16[4,512]{1,0:T(4,128)(2,1)} %tr.1) | copy-start | bytes 12292
  3.8 0.8 %copy-start.9 = (f32[2,4,16]{2,1,0:T(4,128)S(1)}, f32[2,4,16]{2,1,0:T(4,128)}, u32[]{:S(2)}) copy-start(f32[2,4,16]{2,1,0:T(4,128)} %ppre.1) | copy-start | bytes 1540
  3.9 0.8 %copy-start.10 = (f32[1024]{0:T(1024)S(1)}, f32[1024]{0:T(1024)}, u32[]{:S(2)}) copy-start(f32[1024]{0:T(1024)} %param.42) | copy-start | bytes 12292
  3.9 0.8 %copy-start.11 = (s32[2]{0:T(128)S(1)}, s32[2]{0:T(128)}, u32[]{:S(2)}) copy-start(s32[2]{0:T(128)} %acc_s.1) | copy-start | bytes 28
  3.9 0.8 %copy-start.12 = (f32[32]{0:T(128)S(1)}, f32[32]{0:T(128)}, u32[]{:S(2)}) copy-start(f32[32]{0:T(128)} %param.23) | copy-start | bytes 388
  3.9 0.8 %copy-start.13 = (f32[16]{0:T(128)S(1)}, f32[16]{0:T(128)}, u32[]{:S(2)}) copy-start(f32[16]{0:T(128)} %param.35) | copy-start | bytes 196
  3.9 0.8 %copy-start.14 = (f32[16]{0:T(128)S(1)}, f32[16]{0:T(128)}, u32[]{:S(2)}) copy-start(f32[16]{0:T(128)} %param.36) | copy-start | bytes 196
  3.9 0.8 %copy-start.15 = (f32[16]{0:T(128)S(1)}, f32[16]{0:T(128)}, u32[]{:S(2)}) copy-start(f32[16]{0:T(128)} %param.37) | copy-start | bytes 196
  4.8 1.2 %copy-start = (f32[2,16,64,128]{3,2,1,0:T(8,128)S(1)}, f32[2,16,64,128]{3,2,1,0:T(8,128)}, u32[]{:S(2)}) copy-start(f32[2,16,64,128]{3,2,1,0:T(8,128)} %param.41) | copy-start | bytes 3145732

commit v2 on v1

--- a/solution.py
+++ b/solution.py
@@ -26,10 +26,10 @@
     out_ref, st_out,
     hid_v, gain_v, wg_v, wv_v, ww_v, wr_v, ws_v, rawv_v, raww_v, rawr_v, tv_v, tw_v, tr_v, bias_v, rate_v, dgain_v,
     ppre_v, extra_v, prior_v, ngain_v, wo_v,
-    acts_t, wsend, wblk, sblk, acts_f, acts_b, psend, precv, esend, erecv, tot, fsend, frecv, nrm, wog, osend, orecv,
+    acts_t, wsend, wblk, kbuf, qbuf, acts_f, acts_b, psend, precv, esend, erecv, fsend, frecv, nrm, wog, osend, orecv,
     base, state_b,
-    lsem, osem, s1_send, s1_recv, w_send, w_recv, k_send, k_recv, p_send, p_recv, e_send, e_recv, f_send, f_recv,
-    n_send, n_recv, g_send, g_recv, o_send, o_recv, ready,
+    lsem, osem, s1_send, s1_recv, w_send, w_recv, k_send, k_recv, q_send, q_recv, p_send, p_recv, e_send, e_recv,
+    f_send, f_recv, n_send, n_recv, g_send, g_recv, o_send, o_recv, ready,
 ):
     kv = lax.axis_index("kv")
     tp = lax.axis_index("tp")
@@ -47,6 +47,14 @@
             src_ref=src, dst_ref=dst, send_sem=ssem, recv_sem=rsem,
             device_id={"kv": kv_to, "tp": tp_to}, device_id_type=MESH,
         )
+
+    barrier = pltpu.get_barrier_semaphore()
+    for r in range(1, 8):
+        pl.semaphore_signal(barrier, inc=1, device_id={"kv": plane(r), "tp": tp}, device_id_type=MESH)
+    for r in range(1, 8):
+        pl.semaphore_signal(barrier, inc=1, device_id={"kv": ring(r), "tp": tp}, device_id_type=MESH)
+    for r in range(1, 4):
+        pl.semaphore_signal(barrier, inc=1, device_id={"kv": kv, "tp": lax.rem(tp + r, 4)}, device_id_type=MESH)
 
     pairs = [
         (hid, hid_v), (gain, gain_v), (wg, wg_v), (wv, wv_v), (ww, ww_v), (wr, wr_v), (ws, ws_v), (wo, wo_v),
@@ -57,31 +65,25 @@
     for cp in loads:
         cp.start()
 
-    barrier = pltpu.get_barrier_semaphore()
-    for r in range(1, 8):
-        pl.semaphore_signal(barrier, inc=1, device_id={"kv": plane(r), "tp": tp}, device_id_type=MESH)
-    for r in range(1, 8):
-        pl.semaphore_signal(barrier, inc=1, device_id={"kv": ring(r), "tp": tp}, device_id_type=MESH)
-    for r in range(1, 4):
-        pl.semaphore_signal(barrier, inc=1, device_id={"kv": kv, "tp": lax.rem(tp + r, 4)}, device_id_type=MESH)
-
     own32 = pl.ds(pl.multiple_of(c * 32, 32), 32)
     loads[0].wait()
-    acts_t[own32, :] = jnp.transpose(hid_v[...].astype(F32)).astype(BF16)
-    for i in range(1, 7):
-        loads[i].wait()
+    loads[1].wait()
     diag = lax.broadcasted_iota(jnp.int32, (32, 32), 0) == lax.broadcasted_iota(jnp.int32, (32, 32), 1)
     gcol = jnp.sum(jnp.where(diag, jnp.broadcast_to(gain_v[...], (32, 32)), 0.0), axis=1, keepdims=True)
+    hidden = hid_v[...].astype(F32)
+    acts_t[own32, :] = (hidden * gcol).astype(BF16)
+    squares = jnp.sum(hidden * hidden, axis=0, keepdims=True)
+    qbuf[c] = jnp.concatenate([squares[:, i * 128:(i + 1) * 128] for i in range(4)], axis=0)
+    for i in range(2, 7):
+        loads[i].wait()
     for j in range(8):
         lane = slice(j * 128, j * 128 + 128)
-        wsend[j, :, 0:128] = (wg_v[:, lane].astype(F32) * gcol).astype(BF16)
-        wsend[j, :, 128:256] = (wv_v[:, lane].astype(F32) * gcol).astype(BF16)
+        wsend[j, :, 0:128] = wg_v[:, lane]
+        wsend[j, :, 128:256] = wv_v[:, lane]
         half = slice((j % 4) * 128, (j % 4) * 128 + 128)
-        source = ww_v if j < 4 else wr_v
-        wsend[j, :, 256:384] = (source[:, half].astype(F32) * gcol).astype(BF16)
+        wsend[j, :, 256:384] = ww_v[:, half] if j < 4 else wr_v[:, half]
     wblk[own32, :] = wsend[c]
-    step_w = (ws_v[...].astype(F32) * gcol).astype(BF16)
-    sblk[own32, :] = jnp.concatenate([step_w.astype(F32), jnp.zeros((32, 112), F32)], axis=1).astype(BF16)
+    kbuf[c] = jnp.concatenate([ws_v[...].astype(F32), jnp.zeros((16, 96), F32)], axis=1).astype(BF16)
 
     pl.semaphore_wait(barrier, 17)
     for r in range(1, 4):
@@ -96,15 +98,14 @@
         cp = remote(wsend.at[lax.rem(c + r, 8)], wblk.at[own32, :], w_send.at[r], w_recv.at[r], plane(r), tp)
         cp.start()
         w_cp.append(cp)
-        cp = remote(sblk.at[own32, :], sblk.at[own32, :], k_send.at[r], k_recv.at[r], plane(r), tp)
-        cp.start()
-        k_cp.append(cp)
+    for r in range(1, 8):
+        for buf, ssem, rsem in ((kbuf, k_send, k_recv), (qbuf, q_send, q_recv)):
+            cp = remote(buf.at[c], buf.at[c], ssem.at[r], rsem.at[r], plane(r), tp)
+            cp.start()
+            k_cp.append(cp)
 
     loads[7].wait()
-    for i in range(8):
-        wog[z, :, i * 128:(i + 1) * 128] = jnp.transpose(
-            wo_v[i * 128:(i + 1) * 128, :].astype(F32)
-        ).astype(BF16)
+    wog[z] = wo_v[...]
     g_cp = {}
     for r in range(1, 8):
         g_cp[r] = remote(wog.at[z], wog.at[z], g_send.at[r], g_recv.at[r], ring(r), tp)
@@ -125,29 +126,31 @@
         return jnp.where(tok + d < 4, pltpu.roll(x, 8 - d, axis=0), 0.0)
 
     def last_conv(raw, taps):
+        t = taps[...].astype(F32)
+        rows = [raw[k].astype(F32) for k in range(7)]
         parts = []
-        for s in range(2):
-            rows = raw[s].astype(F32)
-            t = taps[...].astype(F32)
-            total = rows[0:4] * t[0:1]
+        for i in range(4):
+            total = rows[i] * t[0:1]
             for j in range(1, 4):
-                total = total + rows[j:j + 4] * t[j:j + 1]
+                total = total + rows[i + j] * t[j:j + 1]
             parts.append(total)
-        return silu(jnp.concatenate(parts, axis=0))
+        return silu(jnp.concatenate([p[s:s + 1] for s in range(2) for p in parts], axis=0))
 
     def base_conv(raw, taps, lo, hi):
         t = taps[...].astype(F32)
-        zero = jnp.zeros((1, hi - lo), F32)
-        rows_out = []
-        for s in range(2):
-            rows = raw[s].astype(F32)
-            a = acc_s[s]
-            win = rows[4:7]
+        rows = [raw[k].astype(F32) for k in range(7)]
+        second = lax.broadcasted_iota(jnp.int32, (2, 1), 0) == 1
+        a = jnp.where(second, acc_s[1], acc_s[0])
+        win = []
+        for i in range(3):
+            w = rows[4 + i]
             for k in range(3, -1, -1):
-                win = jnp.where(a == k, rows[k:k + 3], win)
-            w0, w1, w2 = win[0:1], win[1:2], win[2:3]
-            rows_out += [w0 * t[0:1] + w1 * t[1:2] + w2 * t[2:3], w1 * t[0:1] + w2 * t[1:2], w2 * t[0:1], zero]
-        base[:, lo:hi] = jnp.concatenate(rows_out, axis=0)
+                w = jnp.where(a == k, rows[k + i], w)
+            win.append(w)
+        w0, w1, w2 = win
+        parts = [w0 * t[0:1] + w1 * t[1:2] + w2 * t[2:3], w1 * t[0:1] + w2 * t[1:2], w2 * t[0:1],
+                 jnp.zeros((2, hi - lo), F32)]
+        base[:, lo:hi] = jnp.concatenate([p[s:s + 1] for s in range(2) for p in parts], axis=0)
 
     lastv = last_conv(rawv_v, tv_v)
     lastw = last_conv(raww_v, tw_v)
@@ -202,29 +205,40 @@
         acts_b[i * 128:(i + 1) * 128, :] = block.astype(BF16)
     for cp in w_cp:
         cp.wait_recv()
-    for cp in k_cp:
-        cp.wait_recv()
     p_cp, e_cp = [], []
     for r in Z_ORDER:
         zz = lax.rem(z + r, 8)
         part = jnp.dot(
             acts_b[pl.ds(pl.multiple_of(zz * 64, 64), 64), :], wblk[...], preferred_element_type=F32
         ).astype(BF16)
-        xs = acts_f[pl.ds(pl.multiple_of(zz * 64 + c * 8, 8), 8), :]
-        ext = jnp.dot(xs.astype(BF16), sblk[...], preferred_element_type=F32)
-        ext = jnp.where(lane128 == 16, jnp.sum(xs * xs, axis=1, keepdims=True), ext)
         if r == 0:
             precv[z] = part
-            erecv[z] = ext
         else:
             psend[r] = part
-            esend[r] = ext
             cp = remote(psend.at[r], precv.at[z], p_send.at[r], p_recv.at[r], ring(r), tp)
             cp.start()
             p_cp.append(cp)
-            cp = remote(esend.at[r], erecv.at[z], e_send.at[r], e_recv.at[r], ring(r), tp)
-            cp.start()
-            e_cp.append(cp)
+    for cp in k_cp:
+        cp.wait_recv()
+    own_rows = jnp.concatenate(
+        [acts_f[pl.ds(pl.multiple_of(k * 64 + c * 8, 8), 8), :] for k in range(8)], axis=0
+    ).astype(BF16)
+    step_t = jnp.concatenate([kbuf[j].astype(F32)[:, 0:32] for j in range(8)], axis=1)
+    step_t = jnp.concatenate([step_t, jnp.zeros((112, 256), F32)], axis=0).astype(BF16)
+    turned = (((1,), (1,)), ((), ()))
+    ext = lax.dot_general(own_rows, step_t, turned, preferred_element_type=F32)
+    qsum = qbuf[0]
+    for j in range(1, 8):
+        qsum = qsum + qbuf[j]
+    qeven = pltpu.roll(qsum, 64, axis=1)
+    for k in range(8):
+        row = (qsum if k % 2 else qeven)[k // 2:k // 2 + 1, :]
+        esend[k] = jnp.where(low_half, ext[k * 8:k * 8 + 8, :], jnp.broadcast_to(row, (8, 128)))
+    erecv[z] = esend[z]
+    for r in range(1, 8):
+        cp = remote(esend.at[lax.rem(z + r, 8)], erecv.at[z], e_send.at[r], e_recv.at[r], ring(r), tp)
+        cp.start()
+        e_cp.append(cp)
     for r in (4, 3, 5):
         g_cp[r].start()
 
@@ -233,7 +247,12 @@
     esum = erecv[0]
     for k in range(1, 8):
         esum = esum + erecv[k]
-    inverse = lax.rsqrt(esum[:, 16:17] / 2048.0 + EPS)
+    own_lane = lane128 == 64 + c * 8 + row8
+    inverse = lax.rsqrt(jnp.sum(jnp.where(own_lane, esum, 0.0), axis=1, keepdims=True) / 2048.0 + EPS)
+    lane64 = lax.broadcasted_iota(jnp.int32, (64, 128), 1)
+    row64 = lax.broadcasted_iota(jnp.int32, (64, 128), 0)
+    every = jnp.where(lane64 == 64 + row64, jnp.broadcast_to(esum[0:1, :], (64, 128)), 0.0)
+    inverse64 = lax.rsqrt(jnp.sum(every, axis=1, keepdims=True) / 2048.0 + EPS)
     step = softplus(inverse * esum[:, 0:16] + bias_r)
     decay = rate_e * step + nextra
     cum = decay + down(decay, 1) + down(decay, 2) + down(decay, 3)
@@ -248,6 +267,7 @@
     total = precv[0].astype(F32)
     for k in range(1, 8):
         total = total + precv[k].astype(F32)
+    total = total * inverse64
     for j in range(8):
         rows = total[j * 8:j * 8 + 8, :]
         two = jnp.concatenate(
@@ -268,9 +288,6 @@
     def fresh(j):
         return frecv[j].astype(F32)
 
-    def rounded(x):
-        return (x * inverse).astype(BF16).astype(F32)
-
     def conv(x, lo, taps, at):
         t = taps[:, at:at + 128].astype(F32)
         y = base[:, lo:lo + 128] + x * t[3:4]
@@ -280,8 +297,8 @@
 
     writes, reads = [], []
     for g in range(4):
-        writes.append(conv(rounded(fresh(g)[8:16, 0:128]), 1024 + g * 128, tw_v, g * 128))
-        reads.append(conv(rounded(fresh(4 + g)[8:16, 0:128]), 1536 + g * 128, tr_v, g * 128))
+        writes.append(conv(fresh(g)[8:16, 0:128], 1024 + g * 128, tw_v, g * 128))
+        reads.append(conv(fresh(4 + g)[8:16, 0:128], 1536 + g * 128, tr_v, g * 128))
     carried = []
     for g in range(4):
         rb = reads[g].astype(BF16)
@@ -297,11 +314,11 @@
         for i in range(2):
             j = 2 * g + i
             f = fresh(j)
-            value = conv(rounded(f[0:8, 128:256]), j * 128, tv_v, j * 128)
+            value = conv(f[0:8, 128:256], j * 128, tv_v, j * 128)
             mixed = spread(ecum, j) * carried[g][:, i * 128:(i + 1) * 128] + spread(dg, j) * value
             for d in range(4):
                 mixed = mixed + (inner[d] * spread(pair_w[d], j)) * down(value, d)
-            gated.append(mixed * silu(rounded(f[0:8, 0:128])))
+            gated.append(mixed * silu(f[0:8, 0:128]))
         mean = (jnp.sum(gated[0] * gated[0], axis=1, keepdims=True)
                 + jnp.sum(gated[1] * gated[1], axis=1, keepdims=True)) / 256.0
         scale = lax.rsqrt(mean + EPS)
@@ -323,13 +340,16 @@
     for cp in n_cp:
         cp.wait_recv()
 
-    nall = nrm[...].reshape(128, 512)
+    nall = nrm[...].astype(F32)
     wall = wog[...].reshape(256, 1024)
-    turned = (((1,), (1,)), ((), ()))
-    p0 = lax.dot_general(wall[:, 0:512], nall, turned, preferred_element_type=F32)
-    p1 = lax.dot_general(wall[:, 512:1024], nall, turned, preferred_element_type=F32)
-    both = (p0 + pltpu.roll(p1, 120, axis=1)).astype(BF16)
-    osend[...] = both.reshape(8, 32, 128)
+    p = None
+    for i in range(2):
+        block = nall[:, i * 8:i * 8 + 8, :].reshape(64, 512).astype(BF16)
+        q = lax.dot_general(wall[:, i * 512:(i + 1) * 512], block, turned, preferred_element_type=F32)
+        p = q if p is None else p + q
+    for k in range(8):
+        packed = jnp.concatenate([p[k * 32:k * 32 + 16, :], p[k * 32 + 16:k * 32 + 32, :]], axis=1)
+        osend[k] = packed.astype(BF16)
 
     owner = lax.div(z, 2)
     slot = tp * 2 + lax.rem(z, 2)
@@ -361,10 +381,10 @@
         for x in range(1, 4):
             s4 = s4 + orecv[x * 2 + q].astype(F32)
         sums.append(s4)
-    lane32 = lax.broadcasted_iota(jnp.int32, (32, 128), 1)
-    merged = jnp.transpose(jnp.where(lax.rem(lane32, 16) < 8, sums[0], pltpu.roll(sums[1], 8, axis=1)))
-    ordered = [merged[j * 16 + q * 8:j * 16 + q * 8 + 8, :] for q in range(2) for j in range(8)]
-    out_ref[...] = jnp.concatenate(ordered, axis=0).astype(BF16)
+    lane16 = lax.broadcasted_iota(jnp.int32, (16, 128), 1) < 64
+    top = jnp.where(lane16, sums[0], pltpu.roll(sums[1], 64, axis=1))
+    bottom = jnp.where(lane16, pltpu.roll(sums[0], 64, axis=1), sums[1])
+    out_ref[...] = jnp.concatenate([top, bottom], axis=0).astype(BF16)
 
     state_cp.wait()
     for cp in acts_cp + w_cp + k_cp + p_cp + e_cp + f_cp + n_cp + o_cp + [g_cp[r] for r in range(1, 8)]:
@@ -382,11 +402,12 @@
     group_norm_gain, output_matrix,
 ):
     operands = [
-        hidden_vectors, input_norm_gain.reshape(1, 32), gate_matrix, value_matrix, write_matrix, read_matrix,
-        step_matrix, raw_value_rows, raw_write_rows, raw_read_rows, value_filter_taps, write_filter_taps,
+        hidden_vectors.T, input_norm_gain.reshape(1, 32), gate_matrix, value_matrix, write_matrix, read_matrix,
+        step_matrix.T, raw_value_rows.transpose(1, 0, 2), raw_write_rows.transpose(1, 0, 2),
+        raw_read_rows.transpose(1, 0, 2), value_filter_taps, write_filter_taps,
         read_filter_taps, step_size_bias.reshape(1, 16), rate_logarithm.reshape(1, 16),
         direct_path_gain.reshape(1, 16), prior_step_preact, extra_log_decay, prior_state.reshape(2, 4, 256, 128),
-        group_norm_gain.reshape(1, 1024), output_matrix,
+        group_norm_gain.reshape(1, 1024), output_matrix.T,
     ]
     buffers = [pltpu.VMEM(x.shape, x.dtype) for x in operands]
     dma = pltpu.SemaphoreType.DMA
@@ -394,41 +415,41 @@
         pltpu.VMEM((256, 512), BF16),
         pltpu.VMEM((8, 32, 384), BF16),
         pltpu.VMEM((256, 384), BF16),
-        pltpu.VMEM((256, 128), BF16),
+        pltpu.VMEM((8, 16, 128), BF16),
+        pltpu.VMEM((8, 4, 128), F32),
         pltpu.VMEM((512, 256), F32),
         pltpu.VMEM((512, 256), BF16),
         pltpu.VMEM((8, 64, 384), BF16),
         pltpu.VMEM((8, 64, 384), BF16),
         pltpu.VMEM((8, 8, 128), F32),
         pltpu.VMEM((8, 8, 128), F32),
-        pltpu.VMEM((64, 384), F32),
         pltpu.VMEM((8, 16, 256), BF16),
         pltpu.VMEM((8, 16, 256), BF16),
         pltpu.VMEM((8, 16, 512), BF16),
         pltpu.VMEM((8, 32, 1024), BF16),
-        pltpu.VMEM((8, 32, 128), BF16),
-        pltpu.VMEM((8, 32, 128), BF16),
+        pltpu.VMEM((8, 16, 128), BF16),
+        pltpu.VMEM((8, 16, 128), BF16),
         pltpu.VMEM((8, 2048), F32),
         pltpu.VMEM((2, 4, 256, 128), BF16),
         dma((len(operands),)),
         dma,
-    ] + [dma((8,)) for _ in range(18)] + [pltpu.SemaphoreType.REGULAR]
+    ] + [dma((8,)) for _ in range(20)] + [pltpu.SemaphoreType.REGULAR]
     out, state = pl.pallas_call(
         mixer_kernel,
         out_shape=(
-            jax.ShapeDtypeStruct((128, 32), BF16),
+            jax.ShapeDtypeStruct((32, 128), BF16),
             jax.ShapeDtypeStruct((2, 4, 256, 128), F32),
         ),
         in_specs=[pl.BlockSpec(memory_space=pltpu.SMEM)] + [pl.BlockSpec(memory_space=pl.ANY)] * len(operands),
         out_specs=(pl.BlockSpec(memory_space=pltpu.VMEM), pl.BlockSpec(memory_space=pl.ANY)),
         scratch_shapes=scratch,
         compiler_params=pltpu.CompilerParams(
-            collective_id=0, has_side_effects=True, vmem_limit_bytes=32 * 1024 * 1024
+            collective_id=0, has_side_effects=True, vmem_limit_bytes=67043328
         ),
         cost_estimate=pl.CostEstimate(flops=10**9, bytes_accessed=4 * 10**6, transcendentals=10**5),
         name="mixer",
     )(accepted, *operands)
-    return out, state.reshape(2, 16, 64, 128)
+    return out.T, state.reshape(2, 16, 64, 128)
 
 
 def solution(mesh):

time: 57.1 us -> 54 us (0.946)
  local copies, waits for them, and re-layouts: 6.78 us -> 3.6 us
    unnamed x50 -> x2, local copies, waits for them, and re-layouts: 6.78 us -> 3.6 us
where the time goes in v2:
time: 54 us; the launch traced here: 53.3 us
  Pallas kernels  49 us (91%)
  local copies, waits for them, and re-layouts  3.6 us (7%)
  between operations  0.65 us (1%)
    pallas_call x1, Pallas kernels, per_device(): pl.pallas_call(mixer_kernel, out_shape=(jax.ShapeDtypeStruct((32, 128), B...  49 us
    unnamed x2, local copies, waits for them, and re-layouts  3.6 us

profile of v2, /device:TPU:1, one launch (start us, length us, event | category | flops | bytes accessed | tf_op | source)
XLA Modules:
  0.0 53.3 jit_solution(8698859148707990518)
XLA Ops:
  0.6 49.0 %mixer.1 = (bf16[32,128]{1,0:T(8,128)(2,1)}, f32[2,4,256,128]{3,2,1,0:T(8,128)}) custom-call(s32[2]{0:T(128)} %acc_s.1, bf16[32,512]{1,0:T(8,128)(2,1)} %bitcast.18, f32[1,32]{1,0:T(1,128)} %bitcast.24, bf16[32,1024]{1,0:T(8,128)(2,1)} %wg.1, bf16[32,1024]{1,0:T(8,128)(2,1)} %wv.1, bf16[32,512]{1,0:T(8,128)(2,1)} %ww.1, bf16[32,512]{1,0:T(8,128)(2,1)} %wr.1, ...), custom_call_target="tpu_custom_call" | custom-call | flops 1000000000 | bytes 4000000 | tf_op jit(solution)/shard_map/mixer/pallas_call | solution.py:437
  49.7 1.3 %copy.26 = bf16[128,32]{0,1:T(8,128)(2,1)} copy(bf16[128,32]{0,1:T(8,128)(2,1)} %bitcast.15) | data formatting | bytes 16384
  51.0 2.3 %copy.27 = f32[2,16,64,128]{3,2,1,0:T(8,128)} copy(f32[2,16,64,128]{3,2,1,0:T(8,128)} %bitcast.14) | data formatting | bytes 2097152

commit v3 on v2

--- a/solution.py
+++ b/solution.py
@@ -9,7 +9,7 @@
 F32 = jnp.float32
 BF16 = jnp.bfloat16
 EPS = 1e-6
-Z_ORDER = (4, 3, 5, 2, 6, 1, 7, 0)
+PRIOR = 19
 
 
 def silu(x):
@@ -21,15 +21,14 @@
 
 
 def mixer_kernel(
-    acc_s,
-    hid, gain, wg, wv, ww, wr, ws, rawv, raww, rawr, tv, tw, tr, bias, rate, dgain, ppre, extra, prior, ngain, wo,
+    acc, hid, gain, wg, wv, ww, wr, ws, rawv, raww, rawr, tv, tw, tr, bias, rate, dgain, ppre, extra, prior, ngain, wo,
     out_ref, st_out,
-    hid_v, gain_v, wg_v, wv_v, ww_v, wr_v, ws_v, rawv_v, raww_v, rawr_v, tv_v, tw_v, tr_v, bias_v, rate_v, dgain_v,
-    ppre_v, extra_v, prior_v, ngain_v, wo_v,
-    acts_t, wsend, wblk, kbuf, qbuf, acts_f, acts_b, psend, precv, esend, erecv, fsend, frecv, nrm, wog, osend, orecv,
+    acc_s, hid_v, gain_v, wg_v, wv_v, ww_v, wr_v, ws_v, rawv_v, raww_v, rawr_v, tv_v, tw_v, tr_v, bias_v, rate_v, dgain_v,
+    ppre_v, extra_v, ngain_v, wo_v,
+    acts_t, wsend, wblk, kbuf, qbuf, acts_f, acts_b, psend, arecv, bsend, frecv, esend, erecv, nrm, wog, osend, orecv,
     base, state_b,
-    lsem, osem, s1_send, s1_recv, w_send, w_recv, k_send, k_recv, q_send, q_recv, p_send, p_recv, e_send, e_recv,
-    f_send, f_recv, n_send, n_recv, g_send, g_recv, o_send, o_recv, ready,
+    lsem, s1_send, s1_recv, w_send, w_recv, k_send, k_recv, q_send, q_recv, a_send, a_recv, p_send, p_recv,
+    e_send, e_recv, n_send, n_recv, g_send, g_recv, o_send, o_recv, d_send, d_recv, ready,
 ):
     kv = lax.axis_index("kv")
     tp = lax.axis_index("tp")
@@ -57,62 +56,81 @@
         pl.semaphore_signal(barrier, inc=1, device_id={"kv": kv, "tp": lax.rem(tp + r, 4)}, device_id_type=MESH)
 
     pairs = [
+        (acc, acc_s),
         (hid, hid_v), (gain, gain_v), (wg, wg_v), (wv, wv_v), (ww, ww_v), (wr, wr_v), (ws, ws_v), (wo, wo_v),
         (rawv, rawv_v), (raww, raww_v), (rawr, rawr_v), (tv, tv_v), (tw, tw_v), (tr, tr_v), (bias, bias_v),
-        (rate, rate_v), (dgain, dgain_v), (ppre, ppre_v), (extra, extra_v), (ngain, ngain_v), (prior, prior_v),
+        (rate, rate_v), (dgain, dgain_v), (ppre, ppre_v), (extra, extra_v), (ngain, ngain_v), (prior, st_out),
     ]
     loads = [pltpu.make_async_copy(s, d, lsem.at[i]) for i, (s, d) in enumerate(pairs)]
     for cp in loads:
         cp.start()
 
     own32 = pl.ds(pl.multiple_of(c * 32, 32), 32)
-    loads[0].wait()
     loads[1].wait()
+    loads[2].wait()
     diag = lax.broadcasted_iota(jnp.int32, (32, 32), 0) == lax.broadcasted_iota(jnp.int32, (32, 32), 1)
     gcol = jnp.sum(jnp.where(diag, jnp.broadcast_to(gain_v[...], (32, 32)), 0.0), axis=1, keepdims=True)
     hidden = hid_v[...].astype(F32)
     acts_t[own32, :] = (hidden * gcol).astype(BF16)
     squares = jnp.sum(hidden * hidden, axis=0, keepdims=True)
     qbuf[c] = jnp.concatenate([squares[:, i * 128:(i + 1) * 128] for i in range(4)], axis=0)
-    for i in range(2, 7):
+    for i in range(3, 8):
         loads[i].wait()
     for j in range(8):
         lane = slice(j * 128, j * 128 + 128)
-        wsend[j, :, 0:128] = wg_v[:, lane]
-        wsend[j, :, 128:256] = wv_v[:, lane]
         half = slice((j % 4) * 128, (j % 4) * 128 + 128)
-        wsend[j, :, 256:384] = ww_v[:, half] if j < 4 else wr_v[:, half]
-    wblk[own32, :] = wsend[c]
+        wsend[j, 0] = ww_v[:, half] if j < 4 else wr_v[:, half]
+        wsend[j, 1] = wv_v[:, lane]
+        wsend[j, 2] = wg_v[:, lane]
+    for t in range(3):
+        wblk[t, own32, :] = wsend[c, t]
     kbuf[c] = jnp.concatenate([ws_v[...].astype(F32), jnp.zeros((16, 96), F32)], axis=1).astype(BF16)
 
     pl.semaphore_wait(barrier, 17)
     for r in range(1, 4):
         pl.semaphore_signal(ready, inc=1, device_id={"kv": kv, "tp": lax.rem(tp + r, 4)}, device_id_type=MESH)
 
-    acts_cp, w_cp, k_cp = [], [], []
-    for r in range(1, 8):
-        cp = remote(acts_t.at[own32, :], acts_t.at[own32, :], s1_send.at[r], s1_recv.at[r], plane(r), tp)
+    partner = z * 8 + c + 1 - 2 * lax.rem(c, 2)
+
+    def same_core(i):
+        return pl.ds(pl.multiple_of(lax.rem(c + 8 - 2 * i, 8) * 32, 32), 32)
+
+    acts_cp = [
+        remote(acts_t.at[own32, :], acts_t.at[own32, :], s1_send.at[i], s1_recv.at[i], plane(2 * i) if i else partner, tp)
+        for i in (2, 1, 3, 0)
+    ]
+    for cp in acts_cp:
         cp.start()
-        acts_cp.append(cp)
-    for r in range(1, 8):
-        cp = remote(wsend.at[lax.rem(c + r, 8)], wblk.at[own32, :], w_send.at[r], w_recv.at[r], plane(r), tp)
-        cp.start()
-        w_cp.append(cp)
+    k_cp, w_cp = [], [[], [], []]
     for r in range(1, 8):
         for buf, ssem, rsem in ((kbuf, k_send, k_recv), (qbuf, q_send, q_recv)):
             cp = remote(buf.at[c], buf.at[c], ssem.at[r], rsem.at[r], plane(r), tp)
             cp.start()
             k_cp.append(cp)
-
-    loads[7].wait()
+    for t in range(3):
+        for r in (4, 3, 5, 2, 6, 1, 7):
+            cp = remote(
+                wsend.at[lax.rem(c + r, 8), t], wblk.at[t, own32, :], w_send.at[t, r], w_recv.at[t, r], plane(r), tp
+            )
+            cp.start()
+            w_cp[t].append(cp)
+
+    loads[8].wait()
     wog[z] = wo_v[...]
-    g_cp = {}
-    for r in range(1, 8):
-        g_cp[r] = remote(wog.at[z], wog.at[z], g_send.at[r], g_recv.at[r], ring(r), tp)
-    for r in (2, 6, 1, 7):
-        g_cp[r].start()
-
-    for cp in loads[8:]:
+    g_cp = [[], [], [], []]
+
+    def pass_on(hop):
+        for way, step in ((0, 1), (1, 7)):
+            if hop == 3 and way == 1:
+                continue
+            at = lax.rem(z + 8 * hop - step * hop, 8)
+            cp = remote(wog.at[at], wog.at[at], g_send.at[way, hop], g_recv.at[way, hop], ring(step), tp)
+            cp.start()
+            g_cp[hop].append(cp)
+
+    pass_on(0)
+
+    for cp in loads[:1] + loads[9:]:
         cp.wait()
     row8 = lax.broadcasted_iota(jnp.int32, (8, 1), 0)
     tok = lax.rem(row8, 4)
@@ -191,33 +209,56 @@
                 h = g * 4 + i
                 rows = slice(i * 64, i * 64 + 64)
                 factor = jnp.broadcast_to(etot[s * 4:s * 4 + 1, h:h + 1], (64, 128))
-                new = factor * prior_v[s, g, rows, :] + added[rows, :]
-                prior_v[s, g, rows, :] = new
+                new = factor * st_out[s, g, rows, :] + added[rows, :]
+                st_out[s, g, rows, :] = new
                 state_b[s, g, rows, :] = new.astype(BF16)
-    state_cp = pltpu.make_async_copy(prior_v, st_out, osem)
-    state_cp.start()
-
-    for cp in acts_cp:
+
+    d_cp = []
+    for i in (1, 3, 2):
+        remote(acts_t.at[own32, :], acts_t.at[own32, :], s1_send.at[i], s1_recv.at[i], partner, tp).wait_recv()
+        cp = remote(acts_t.at[same_core(i), :], acts_t.at[same_core(i), :], d_send.at[i], d_recv.at[i], partner, tp)
+        cp.start()
+        d_cp.append(cp)
+    for cp in g_cp[0]:
+        cp.wait_recv()
+    pass_on(1)
+    remote(acts_t.at[own32, :], acts_t.at[own32, :], s1_send.at[0], s1_recv.at[0], partner, tp).wait_recv()
+    for cp in d_cp:
         cp.wait_recv()
     for i in range(4):
         block = jnp.transpose(acts_t[:, i * 128:(i + 1) * 128].astype(F32))
         acts_f[i * 128:(i + 1) * 128, :] = block
         acts_b[i * 128:(i + 1) * 128, :] = block.astype(BF16)
-    for cp in w_cp:
-        cp.wait_recv()
-    p_cp, e_cp = [], []
-    for r in Z_ORDER:
-        zz = lax.rem(z + r, 8)
-        part = jnp.dot(
-            acts_b[pl.ds(pl.multiple_of(zz * 64, 64), 64), :], wblk[...], preferred_element_type=F32
-        ).astype(BF16)
-        if r == 0:
-            precv[z] = part
-        else:
-            psend[r] = part
-            cp = remote(psend.at[r], precv.at[z], p_send.at[r], p_recv.at[r], ring(r), tp)
+    turned = (((1,), (1,)), ((), ()))
+    even = lax.rem(z, 2) == 0
+    far = lax.rem(z + 2 + 4 * lax.rem(z, 2), 8)
+    a_cp, p_cp = [[], [], []], []
+
+    def to_owners(t, src, slot, dz, skip_self):
+        for r in range(1 if skip_self else 0, 8):
+            cc = lax.rem(c + r, 8)
+            cp = remote(
+                src.at[cc], frecv.at[t, slot, c], p_send.at[t, slot, r], p_recv.at[t, slot, r],
+                lax.rem(z + dz, 8) * 8 + cc, tp,
+            )
             cp.start()
-            p_cp.append(cp)
+            p_cp.append((t, cp))
+
+    for t in range(3):
+        for cp in w_cp[t]:
+            cp.wait_recv()
+        part = jnp.dot(acts_b[...], wblk[t], preferred_element_type=F32)
+        psend[t] = part.reshape(8, 8, 8, 128).astype(BF16)
+        for kind, away, to in ((2, 4, far * 8 + c), (0, 3, ring(1)), (1, 5, ring(7))):
+            cp = remote(
+                psend.at[t, lax.rem(z + away, 8)], arecv.at[t, kind], a_send.at[t, kind], a_recv.at[t, kind], to, tp
+            )
+            cp.start()
+            a_cp[t].append(cp)
+        to_owners(t, psend.at[t, lax.rem(z + 1, 8)], 1, 1, False)
+        to_owners(t, psend.at[t, lax.rem(z + 7, 8)], 2, 7, False)
+        to_owners(t, psend.at[t, z], 0, 0, True)
+        frecv[t, 0, c] = psend[t, z, c]
     for cp in k_cp:
         cp.wait_recv()
     own_rows = jnp.concatenate(
@@ -225,7 +266,6 @@
     ).astype(BF16)
     step_t = jnp.concatenate([kbuf[j].astype(F32)[:, 0:32] for j in range(8)], axis=1)
     step_t = jnp.concatenate([step_t, jnp.zeros((112, 256), F32)], axis=0).astype(BF16)
-    turned = (((1,), (1,)), ((), ()))
     ext = lax.dot_general(own_rows, step_t, turned, preferred_element_type=F32)
     qsum = qbuf[0]
     for j in range(1, 8):
@@ -233,26 +273,41 @@
     qeven = pltpu.roll(qsum, 64, axis=1)
     for k in range(8):
         row = (qsum if k % 2 else qeven)[k // 2:k // 2 + 1, :]
-        esend[k] = jnp.where(low_half, ext[k * 8:k * 8 + 8, :], jnp.broadcast_to(row, (8, 128)))
+        mixture = jnp.where(low_half, ext[k * 8:k * 8 + 8, :], jnp.broadcast_to(row, (8, 128)))
+        high = mixture.astype(BF16).astype(F32)
+        rest = (mixture - high).astype(BF16).astype(F32)
+        lower = jnp.where(low_half, pltpu.roll(jnp.where(low_half, rest, 0.0), 16, axis=1), rest)
+        esend[k] = jnp.where(low_half, high + lower, jnp.where(row8 < 4, high, lower)).astype(BF16)
     erecv[z] = esend[z]
-    for r in range(1, 8):
+    e_cp = []
+    for r in (4, 3, 5, 2, 6, 1, 7):
         cp = remote(esend.at[lax.rem(z + r, 8)], erecv.at[z], e_send.at[r], e_recv.at[r], ring(r), tp)
         cp.start()
         e_cp.append(cp)
-    for r in (4, 3, 5):
-        g_cp[r].start()
+    for cp in g_cp[1]:
+        cp.wait_recv()
+    for t in range(3):
+        for cp in a_cp[t]:
+            cp.wait_recv()
+        extra_block = arecv[t, 2].astype(F32)
+        zero_block = jnp.zeros_like(extra_block)
+        plus = psend[t, lax.rem(z + 2, 8)].astype(F32) + arecv[t, 0].astype(F32)
+        minus = psend[t, lax.rem(z + 6, 8)].astype(F32) + arecv[t, 1].astype(F32)
+        bsend[t, 0] = (plus + jnp.where(even, extra_block, zero_block)).astype(BF16)
+        bsend[t, 1] = (minus + jnp.where(even, zero_block, extra_block)).astype(BF16)
+        to_owners(t, bsend.at[t, 0], 3, 2, False)
+        to_owners(t, bsend.at[t, 1], 4, 6, False)
+    pass_on(2)
 
     for cp in e_cp:
         cp.wait_recv()
-    esum = erecv[0]
+    esum = erecv[0].astype(F32)
     for k in range(1, 8):
-        esum = esum + erecv[k]
+        esum = esum + erecv[k].astype(F32)
     own_lane = lane128 == 64 + c * 8 + row8
-    inverse = lax.rsqrt(jnp.sum(jnp.where(own_lane, esum, 0.0), axis=1, keepdims=True) / 2048.0 + EPS)
-    lane64 = lax.broadcasted_iota(jnp.int32, (64, 128), 1)
-    row64 = lax.broadcasted_iota(jnp.int32, (64, 128), 0)
-    every = jnp.where(lane64 == 64 + row64, jnp.broadcast_to(esum[0:1, :], (64, 128)), 0.0)
-    inverse64 = lax.rsqrt(jnp.sum(every, axis=1, keepdims=True) / 2048.0 + EPS)
+    qrow = jnp.broadcast_to(esum[0:1, :] + esum[4:5, :], (8, 128))
+    inverse = lax.rsqrt(jnp.sum(jnp.where(own_lane, qrow, 0.0), axis=1, keepdims=True) / 2048.0 + EPS)
+    esum = esum + pltpu.roll(esum, 112, axis=1)
     step = softplus(inverse * esum[:, 0:16] + bias_r)
     decay = rate_e * step + nextra
     cum = decay + down(decay, 1) + down(decay, 2) + down(decay, 3)
@@ -262,31 +317,19 @@
         pair_w.append(jnp.where(tok >= d, w, 0.0))
     ecum = jnp.exp(cum)
 
-    for cp in p_cp:
-        cp.wait_recv()
-    total = precv[0].astype(F32)
-    for k in range(1, 8):
-        total = total + precv[k].astype(F32)
-    total = total * inverse64
-    for j in range(8):
-        rows = total[j * 8:j * 8 + 8, :]
-        two = jnp.concatenate(
-            [rows[:, 0:256], jnp.concatenate([rows[:, 256:384], rows[:, 256:384]], axis=1)], axis=0
-        )
-        fsend[j] = two.astype(BF16)
-    frecv[c] = fsend[c]
-    f_cp = []
-    for r in range(1, 8):
-        cp = remote(fsend.at[lax.rem(c + r, 8)], frecv.at[c], f_send.at[r], f_recv.at[r], plane(r), tp)
-        cp.start()
-        f_cp.append(cp)
+    def settle(t):
+        for at, cp in p_cp:
+            if at == t:
+                cp.wait_recv()
+
+    def fresh(t, j):
+        x = frecv[t, 0, j].astype(F32)
+        for slot in range(1, 5):
+            x = x + frecv[t, slot, j].astype(F32)
+        return (x * inverse).astype(BF16).astype(F32)
 
     dg = jnp.broadcast_to(dgain_v[...], (8, 16))
-    for cp in f_cp:
-        cp.wait_recv()
-
-    def fresh(j):
-        return frecv[j].astype(F32)
+    settle(0)
 
     def conv(x, lo, taps, at):
         t = taps[:, at:at + 128].astype(F32)
@@ -295,32 +338,30 @@
             y = y + down(x, d) * t[3 - d:4 - d]
         return silu(y)
 
-    writes, reads = [], []
-    for g in range(4):
-        writes.append(conv(fresh(g)[8:16, 0:128], 1024 + g * 128, tw_v, g * 128))
-        reads.append(conv(fresh(4 + g)[8:16, 0:128], 1536 + g * 128, tr_v, g * 128))
-    carried = []
+    writes = [conv(fresh(0, g), 1024 + g * 128, tw_v, g * 128) for g in range(4)]
+    reads = [conv(fresh(0, 4 + g), 1536 + g * 128, tr_v, g * 128) for g in range(4)]
+    carried, inner = [], []
     for g in range(4):
         rb = reads[g].astype(BF16)
         both = [
-            lax.dot_general(rb, state_b[s, g], (((1,), (1,)), ((), ())), preferred_element_type=F32)
-            for s in range(2)
+            lax.dot_general(rb, state_b[s, g], turned, preferred_element_type=F32) for s in range(2)
         ]
         carried.append(jnp.where(row8 < 4, both[0], both[1]))
+        inner.append([jnp.sum(reads[g] * down(writes[g], d), axis=1, keepdims=True) for d in range(4)])
+    settle(1)
+    mixed = []
+    for j in range(8):
+        g, i = j // 2, j % 2
+        value = conv(fresh(1, j), j * 128, tv_v, j * 128)
+        m = spread(ecum, j) * carried[g][:, i * 128:(i + 1) * 128] + spread(dg, j) * value
+        for d in range(4):
+            m = m + (inner[g][d] * spread(pair_w[d], j)) * down(value, d)
+        mixed.append(m)
+    settle(2)
     normed = []
     for g in range(4):
-        inner = [jnp.sum(reads[g] * down(writes[g], d), axis=1, keepdims=True) for d in range(4)]
-        gated = []
-        for i in range(2):
-            j = 2 * g + i
-            f = fresh(j)
-            value = conv(f[0:8, 128:256], j * 128, tv_v, j * 128)
-            mixed = spread(ecum, j) * carried[g][:, i * 128:(i + 1) * 128] + spread(dg, j) * value
-            for d in range(4):
-                mixed = mixed + (inner[d] * spread(pair_w[d], j)) * down(value, d)
-            gated.append(mixed * silu(f[0:8, 0:128]))
-        mean = (jnp.sum(gated[0] * gated[0], axis=1, keepdims=True)
-                + jnp.sum(gated[1] * gated[1], axis=1, keepdims=True)) / 256.0
+        gated = [mixed[j] * silu(fresh(2, j)) for j in (2 * g, 2 * g + 1)]
+        mean = jnp.sum(gated[0] * gated[0] + gated[1] * gated[1], axis=1, keepdims=True) / 256.0
         scale = lax.rsqrt(mean + EPS)
         for i in range(2):
             j = 2 * g + i
@@ -334,8 +375,11 @@
         cp = remote(nrm.at[c], nrm.at[c], n_send.at[r], n_recv.at[r], plane(r), tp)
         cp.start()
         n_cp.append(cp)
-    for r in range(1, 8):
-        g_cp[r].wait_recv()
+    for cp in g_cp[2]:
+        cp.wait_recv()
+    pass_on(3)
+    for cp in g_cp[3]:
+        cp.wait_recv()
     pl.semaphore_wait(ready, 3)
     for cp in n_cp:
         cp.wait_recv()
@@ -386,9 +430,9 @@
     bottom = jnp.where(lane16, pltpu.roll(sums[0], 64, axis=1), sums[1])
     out_ref[...] = jnp.concatenate([top, bottom], axis=0).astype(BF16)
 
-    state_cp.wait()
-    for cp in acts_cp + w_cp + k_cp + p_cp + e_cp + f_cp + n_cp + o_cp + [g_cp[r] for r in range(1, 8)]:
-        cp.wait_send()
+    for group in [acts_cp, d_cp, k_cp, e_cp, n_cp, o_cp, [cp for _, cp in p_cp]] + w_cp + a_cp + g_cp:
+        for cp in group:
+            cp.wait_send()
 
     @pl.when(owner != tp)
     def _():
@@ -402,29 +446,31 @@
     group_norm_gain, output_matrix,
 ):
     operands = [
-        hidden_vectors.T, input_norm_gain.reshape(1, 32), gate_matrix, value_matrix, write_matrix, read_matrix,
+        accepted, hidden_vectors.T, input_norm_gain.reshape(1, 32), gate_matrix, value_matrix, write_matrix, read_matrix,
         step_matrix.T, raw_value_rows.transpose(1, 0, 2), raw_write_rows.transpose(1, 0, 2),
         raw_read_rows.transpose(1, 0, 2), value_filter_taps, write_filter_taps,
         read_filter_taps, step_size_bias.reshape(1, 16), rate_logarithm.reshape(1, 16),
         direct_path_gain.reshape(1, 16), prior_step_preact, extra_log_decay, prior_state.reshape(2, 4, 256, 128),
         group_norm_gain.reshape(1, 1024), output_matrix.T,
     ]
-    buffers = [pltpu.VMEM(x.shape, x.dtype) for x in operands]
+    buffers = [pltpu.SMEM((2,), jnp.int32)] + [
+        pltpu.VMEM(x.shape, x.dtype) for i, x in enumerate(operands) if i not in (0, PRIOR)
+    ]
     dma = pltpu.SemaphoreType.DMA
     scratch = buffers + [
         pltpu.VMEM((256, 512), BF16),
-        pltpu.VMEM((8, 32, 384), BF16),
-        pltpu.VMEM((256, 384), BF16),
+        pltpu.VMEM((8, 3, 32, 128), BF16),
+        pltpu.VMEM((3, 256, 128), BF16),
         pltpu.VMEM((8, 16, 128), BF16),
         pltpu.VMEM((8, 4, 128), F32),
         pltpu.VMEM((512, 256), F32),
         pltpu.VMEM((512, 256), BF16),
-        pltpu.VMEM((8, 64, 384), BF16),
-        pltpu.VMEM((8, 64, 384), BF16),
-        pltpu.VMEM((8, 8, 128), F32),
-        pltpu.VMEM((8, 8, 128), F32),
-        pltpu.VMEM((8, 16, 256), BF16),
-        pltpu.VMEM((8, 16, 256), BF16),
+        pltpu.VMEM((3, 8, 8, 8, 128), BF16),
+        pltpu.VMEM((3, 3, 8, 8, 128), BF16),
+        pltpu.VMEM((3, 2, 8, 8, 128), BF16),
+        pltpu.VMEM((3, 5, 8, 8, 128), BF16),
+        pltpu.VMEM((8, 8, 128), BF16),
+        pltpu.VMEM((8, 8, 128), BF16),
         pltpu.VMEM((8, 16, 512), BF16),
         pltpu.VMEM((8, 32, 1024), BF16),
         pltpu.VMEM((8, 16, 128), BF16),
@@ -432,23 +478,34 @@
         pltpu.VMEM((8, 2048), F32),
         pltpu.VMEM((2, 4, 256, 128), BF16),
         dma((len(operands),)),
-        dma,
-    ] + [dma((8,)) for _ in range(20)] + [pltpu.SemaphoreType.REGULAR]
+        dma((4,)), dma((4,)),
+        dma((3, 8)), dma((3, 8)),
+        dma((8,)), dma((8,)), dma((8,)), dma((8,)),
+        dma((3, 3)), dma((3, 3)),
+        dma((3, 5, 8)), dma((3, 5, 8)),
+        dma((8,)), dma((8,)),
+        dma((8,)), dma((8,)),
+        dma((2, 4)), dma((2, 4)),
+        dma((8,)), dma((8,)),
+        dma((4,)), dma((4,)),
+        pltpu.SemaphoreType.REGULAR,
+    ]
+    operands = [pltpu.with_memory_space_constraint(x, pltpu.HBM) for x in operands]
     out, state = pl.pallas_call(
         mixer_kernel,
         out_shape=(
-            jax.ShapeDtypeStruct((32, 128), BF16),
-            jax.ShapeDtypeStruct((2, 4, 256, 128), F32),
+            pltpu.VMEM((32, 128), BF16),
+            pltpu.VMEM((2, 4, 256, 128), F32),
         ),
-        in_specs=[pl.BlockSpec(memory_space=pltpu.SMEM)] + [pl.BlockSpec(memory_space=pl.ANY)] * len(operands),
-        out_specs=(pl.BlockSpec(memory_space=pltpu.VMEM), pl.BlockSpec(memory_space=pl.ANY)),
+        in_specs=[pl.BlockSpec(memory_space=pl.ANY)] * len(operands),
+        out_specs=(pl.BlockSpec(memory_space=pltpu.VMEM), pl.BlockSpec(memory_space=pltpu.VMEM)),
         scratch_shapes=scratch,
         compiler_params=pltpu.CompilerParams(
-            collective_id=0, has_side_effects=True, vmem_limit_bytes=67043328
+            collective_id=0, has_side_effects=True, vmem_limit_bytes=32 * 1024 * 1024
         ),
         cost_estimate=pl.CostEstimate(flops=10**9, bytes_accessed=4 * 10**6, transcendentals=10**5),
         name="mixer",
-    )(accepted, *operands)
+    )(*operands)
     return out.T, state.reshape(2, 16, 64, 128)
 
 

time: 54 us -> 42 us (0.78); the launches traced: 53.3 us -> 41.9 us
  Pallas kernels: 49 us -> 39.7 us
  local copies, waits for them, and re-layouts: 3.6 us -> 1.57 us
    pallas_call x1, Pallas kernels: 49 us -> 39.7 us  [per_device(): pl.pallas_call(mixer_kernel, out_shape=(pltpu.VMEM((32, 128), BF16), pltp...]
    unnamed x2, local copies, waits for them, and re-layouts: 3.6 us -> 1.57 us
where the time goes in v3:
time: 42 us; the launch traced here: 41.9 us
  Pallas kernels  39.7 us (95%)
  local copies, waits for them, and re-layouts  1.57 us (4%)
  between operations  0.65 us (2%)
    pallas_call x1, Pallas kernels, per_device(): pl.pallas_call(mixer_kernel, out_shape=(pltpu.VMEM((32, 128), BF16), pltp...  39.7 us
    unnamed x2, local copies, waits for them, and re-layouts  1.57 us

profile of v3, /device:TPU:1, one launch (start us, length us, event | category | flops | bytes accessed | tf_op | source)
XLA Modules:
  0.0 41.9 jit_solution(10049307107912092669)
XLA Ops:
  0.6 39.7 %mixer.1 = (bf16[32,128]{1,0:T(8,128)(2,1)S(1)}, f32[2,4,256,128]{3,2,1,0:T(8,128)S(1)}) custom-call(s32[2]{0:T(128)} %acc.1, bf16[32,512]{1,0:T(8,128)(2,1)} %bitcast.18, f32[1,32]{1,0:T(1,128)} %bitcast.24, bf16[32,1024]{1,0:T(8,128)(2,1)} %wg.1, bf16[32,1024]{1,0:T(8,128)(2,1)} %wv.1, bf16[32,512]{1,0:T(8,128)(2,1)} %ww.1, bf16[32,512]{1,0:T(8,128)(2,1)} %wr.1, ...), custom_call_target="tpu_custom_call" | custom-call | flops 1000000000 | bytes 4000000 | tf_op jit(solution)/shard_map/mixer/pallas_call | solution.py:494
  40.3 0.6 %copy.26 = bf16[128,32]{0,1:T(8,128)(2,1)} copy(bf16[128,32]{0,1:T(8,128)(2,1)S(1)} %bitcast.15) | data formatting | bytes 16384
  40.9 1.0 %copy.27 = f32[2,16,64,128]{3,2,1,0:T(8,128)} copy(f32[2,16,64,128]{3,2,1,0:T(8,128)S(1)} %bitcast.14) | data formatting | bytes 2097152

commit v4 on v3

--- a/solution.py
+++ b/solution.py
@@ -27,8 +27,8 @@
     ppre_v, extra_v, ngain_v, wo_v,
     acts_t, wsend, wblk, kbuf, qbuf, acts_f, acts_b, psend, arecv, bsend, frecv, esend, erecv, nrm, wog, osend, orecv,
     base, state_b,
-    lsem, s1_send, s1_recv, w_send, w_recv, k_send, k_recv, q_send, q_recv, a_send, a_recv, p_send, p_recv,
-    e_send, e_recv, n_send, n_recv, g_send, g_recv, o_send, o_recv, d_send, d_recv, ready,
+    lsem, acts_ssem, acts_rsem, d_ssem, d_rsem, w_ssem, w_rsem, k_ssem, k_rsem, q_ssem, q_rsem, g_ssem, g_rsem,
+    a_ssem, a_rsem, p_ssem, p_rsem, h_ssem, h_rsem, e_ssem, e_rsem, n_ssem, n_rsem, o_ssem, o_rsem, ready,
 ):
     kv = lax.axis_index("kv")
     tp = lax.axis_index("tp")
@@ -46,6 +46,12 @@
             src_ref=src, dst_ref=dst, send_sem=ssem, recv_sem=rsem,
             device_id={"kv": kv_to, "tp": tp_to}, device_id_type=MESH,
         )
+
+    def arrived(ref, sem):
+        remote(ref, ref, acts_ssem, sem, kv, tp).wait_recv()
+
+    def sent(ref, sem):
+        remote(ref, ref, sem, d_rsem, kv, tp).wait_send()
 
     barrier = pltpu.get_barrier_semaphore()
     for r in range(1, 8):
@@ -95,38 +101,26 @@
     def same_core(i):
         return pl.ds(pl.multiple_of(lax.rem(c + 8 - 2 * i, 8) * 32, 32), 32)
 
-    acts_cp = [
-        remote(acts_t.at[own32, :], acts_t.at[own32, :], s1_send.at[i], s1_recv.at[i], plane(2 * i) if i else partner, tp)
-        for i in (2, 1, 3, 0)
-    ]
-    for cp in acts_cp:
-        cp.start()
-    k_cp, w_cp = [], [[], [], []]
-    for r in range(1, 8):
-        for buf, ssem, rsem in ((kbuf, k_send, k_recv), (qbuf, q_send, q_recv)):
-            cp = remote(buf.at[c], buf.at[c], ssem.at[r], rsem.at[r], plane(r), tp)
-            cp.start()
-            k_cp.append(cp)
+    for i in (2, 1, 3):
+        remote(acts_t.at[own32, :], acts_t.at[own32, :], acts_ssem, acts_rsem.at[i], plane(2 * i), tp).start()
+    remote(acts_t.at[own32, :], acts_t.at[own32, :], acts_ssem, d_rsem, partner, tp).start()
     for t in range(3):
         for r in (4, 3, 5, 2, 6, 1, 7):
-            cp = remote(
-                wsend.at[lax.rem(c + r, 8), t], wblk.at[t, own32, :], w_send.at[t, r], w_recv.at[t, r], plane(r), tp
-            )
-            cp.start()
-            w_cp[t].append(cp)
+            remote(wsend.at[lax.rem(c + r, 8), t], wblk.at[t, own32, :], w_ssem, w_rsem.at[t], plane(r), tp).start()
+        if t == 0:
+            for r in (4, 3, 5, 2, 6, 1, 7):
+                remote(kbuf.at[c], kbuf.at[c], k_ssem, k_rsem, plane(r), tp).start()
+                remote(qbuf.at[c], qbuf.at[c], q_ssem, q_rsem, plane(r), tp).start()
 
     loads[8].wait()
     wog[z] = wo_v[...]
-    g_cp = [[], [], [], []]
 
     def pass_on(hop):
         for way, step in ((0, 1), (1, 7)):
             if hop == 3 and way == 1:
                 continue
             at = lax.rem(z + 8 * hop - step * hop, 8)
-            cp = remote(wog.at[at], wog.at[at], g_send.at[way, hop], g_recv.at[way, hop], ring(step), tp)
-            cp.start()
-            g_cp[hop].append(cp)
+            remote(wog.at[at], wog.at[at], g_ssem, g_rsem.at[hop], ring(step), tp).start()
 
     pass_on(0)
 
@@ -213,18 +207,12 @@
                 st_out[s, g, rows, :] = new
                 state_b[s, g, rows, :] = new.astype(BF16)
 
-    d_cp = []
     for i in (1, 3, 2):
-        remote(acts_t.at[own32, :], acts_t.at[own32, :], s1_send.at[i], s1_recv.at[i], partner, tp).wait_recv()
-        cp = remote(acts_t.at[same_core(i), :], acts_t.at[same_core(i), :], d_send.at[i], d_recv.at[i], partner, tp)
-        cp.start()
-        d_cp.append(cp)
-    for cp in g_cp[0]:
-        cp.wait_recv()
+        arrived(acts_t.at[own32, :], acts_rsem.at[i])
+        remote(acts_t.at[same_core(i), :], acts_t.at[same_core(i), :], d_ssem, d_rsem, partner, tp).start()
+    arrived(wog.at[0:2], g_rsem.at[0])
     pass_on(1)
-    remote(acts_t.at[own32, :], acts_t.at[own32, :], s1_send.at[0], s1_recv.at[0], partner, tp).wait_recv()
-    for cp in d_cp:
-        cp.wait_recv()
+    arrived(acts_t.at[0:128, :], d_rsem)
     for i in range(4):
         block = jnp.transpose(acts_t[:, i * 128:(i + 1) * 128].astype(F32))
         acts_f[i * 128:(i + 1) * 128, :] = block
@@ -232,35 +220,24 @@
     turned = (((1,), (1,)), ((), ()))
     even = lax.rem(z, 2) == 0
     far = lax.rem(z + 2 + 4 * lax.rem(z, 2), 8)
-    a_cp, p_cp = [[], [], []], []
-
-    def to_owners(t, src, slot, dz, skip_self):
-        for r in range(1 if skip_self else 0, 8):
+
+    def to_owners(src, t, slot, dz, ssem, rsem):
+        for r in range(0 if dz else 1, 8):
             cc = lax.rem(c + r, 8)
-            cp = remote(
-                src.at[cc], frecv.at[t, slot, c], p_send.at[t, slot, r], p_recv.at[t, slot, r],
-                lax.rem(z + dz, 8) * 8 + cc, tp,
-            )
-            cp.start()
-            p_cp.append((t, cp))
+            remote(src.at[cc], frecv.at[t, slot, c], ssem, rsem, lax.rem(z + dz, 8) * 8 + cc, tp).start()
 
     for t in range(3):
-        for cp in w_cp[t]:
-            cp.wait_recv()
+        arrived(wblk.at[t, 0:224, :], w_rsem.at[t])
         part = jnp.dot(acts_b[...], wblk[t], preferred_element_type=F32)
         psend[t] = part.reshape(8, 8, 8, 128).astype(BF16)
         for kind, away, to in ((2, 4, far * 8 + c), (0, 3, ring(1)), (1, 5, ring(7))):
-            cp = remote(
-                psend.at[t, lax.rem(z + away, 8)], arecv.at[t, kind], a_send.at[t, kind], a_recv.at[t, kind], to, tp
-            )
-            cp.start()
-            a_cp[t].append(cp)
-        to_owners(t, psend.at[t, lax.rem(z + 1, 8)], 1, 1, False)
-        to_owners(t, psend.at[t, lax.rem(z + 7, 8)], 2, 7, False)
-        to_owners(t, psend.at[t, z], 0, 0, True)
+            remote(psend.at[t, lax.rem(z + away, 8)], arecv.at[t, kind], a_ssem, a_rsem.at[t], to, tp).start()
+        to_owners(psend.at[t, lax.rem(z + 1, 8)], t, 1, 1, p_ssem, p_rsem.at[t])
+        to_owners(psend.at[t, lax.rem(z + 7, 8)], t, 2, 7, p_ssem, p_rsem.at[t])
+        to_owners(psend.at[t, z], t, 0, 0, h_ssem, h_rsem.at[t])
         frecv[t, 0, c] = psend[t, z, c]
-    for cp in k_cp:
-        cp.wait_recv()
+    arrived(kbuf.at[0:7], k_rsem)
+    arrived(qbuf.at[0:7], q_rsem)
     own_rows = jnp.concatenate(
         [acts_f[pl.ds(pl.multiple_of(k * 64 + c * 8, 8), 8), :] for k in range(8)], axis=0
     ).astype(BF16)
@@ -279,28 +256,22 @@
         lower = jnp.where(low_half, pltpu.roll(jnp.where(low_half, rest, 0.0), 16, axis=1), rest)
         esend[k] = jnp.where(low_half, high + lower, jnp.where(row8 < 4, high, lower)).astype(BF16)
     erecv[z] = esend[z]
-    e_cp = []
     for r in (4, 3, 5, 2, 6, 1, 7):
-        cp = remote(esend.at[lax.rem(z + r, 8)], erecv.at[z], e_send.at[r], e_recv.at[r], ring(r), tp)
-        cp.start()
-        e_cp.append(cp)
-    for cp in g_cp[1]:
-        cp.wait_recv()
+        remote(esend.at[lax.rem(z + r, 8)], erecv.at[z], e_ssem, e_rsem, ring(r), tp).start()
+    arrived(wog.at[0:2], g_rsem.at[1])
     for t in range(3):
-        for cp in a_cp[t]:
-            cp.wait_recv()
+        arrived(arecv.at[t], a_rsem.at[t])
         extra_block = arecv[t, 2].astype(F32)
         zero_block = jnp.zeros_like(extra_block)
         plus = psend[t, lax.rem(z + 2, 8)].astype(F32) + arecv[t, 0].astype(F32)
         minus = psend[t, lax.rem(z + 6, 8)].astype(F32) + arecv[t, 1].astype(F32)
         bsend[t, 0] = (plus + jnp.where(even, extra_block, zero_block)).astype(BF16)
         bsend[t, 1] = (minus + jnp.where(even, zero_block, extra_block)).astype(BF16)
-        to_owners(t, bsend.at[t, 0], 3, 2, False)
-        to_owners(t, bsend.at[t, 1], 4, 6, False)
+        to_owners(bsend.at[t, 0], t, 3, 2, p_ssem, p_rsem.at[t])
+        to_owners(bsend.at[t, 1], t, 4, 6, p_ssem, p_rsem.at[t])
     pass_on(2)
 
-    for cp in e_cp:
-        cp.wait_recv()
+    arrived(erecv.at[0:7], e_rsem)
     esum = erecv[0].astype(F32)
     for k in range(1, 8):
         esum = esum + erecv[k].astype(F32)
@@ -318,9 +289,8 @@
     ecum = jnp.exp(cum)
 
     def settle(t):
-        for at, cp in p_cp:
-            if at == t:
-                cp.wait_recv()
+        arrived(frecv.at[t, 1:5], p_rsem.at[t])
+        arrived(frecv.at[t, 0, 0:7], h_rsem.at[t])
 
     def fresh(t, j):
         x = frecv[t, 0, j].astype(F32)
@@ -370,19 +340,13 @@
         [jnp.concatenate(normed[0:4], axis=1), jnp.concatenate(normed[4:8], axis=1)], axis=0
     ).astype(BF16)
 
-    n_cp = []
-    for r in range(1, 8):
-        cp = remote(nrm.at[c], nrm.at[c], n_send.at[r], n_recv.at[r], plane(r), tp)
-        cp.start()
-        n_cp.append(cp)
-    for cp in g_cp[2]:
-        cp.wait_recv()
+    for r in (4, 3, 5, 2, 6, 1, 7):
+        remote(nrm.at[c], nrm.at[c], n_ssem, n_rsem, plane(r), tp).start()
+    arrived(wog.at[0:2], g_rsem.at[2])
     pass_on(3)
-    for cp in g_cp[3]:
-        cp.wait_recv()
+    arrived(wog.at[0], g_rsem.at[3])
     pl.semaphore_wait(ready, 3)
-    for cp in n_cp:
-        cp.wait_recv()
+    arrived(nrm.at[0:7], n_rsem)
 
     nall = nrm[...].astype(F32)
     wall = wog[...].reshape(256, 1024)
@@ -397,27 +361,18 @@
 
     owner = lax.div(z, 2)
     slot = tp * 2 + lax.rem(z, 2)
-    o_cp = []
     for r in (4, 3, 5, 2, 6, 1, 7):
-        cp = remote(osend.at[lax.rem(z + r, 8)], orecv.at[slot], o_send.at[r], o_recv.at[slot], ring(r), owner)
-        cp.start()
-        o_cp.append(cp)
-    straight = remote(osend.at[z], orecv.at[slot], o_send.at[0], o_recv.at[slot], kv, owner)
+        remote(osend.at[lax.rem(z + r, 8)], orecv.at[slot], o_ssem, o_rsem, ring(r), owner).start()
 
     @pl.when(owner != tp)
     def _():
-        straight.start()
+        remote(osend.at[z], orecv.at[slot], o_ssem, o_rsem, kv, owner).start()
+        arrived(orecv.at[0:8], o_rsem)
 
     @pl.when(owner == tp)
     def _():
         orecv[slot] = osend[z]
-
-    for i in range(8):
-        mine = jnp.logical_and(tp == i // 2, z == tp * 2 + i % 2)
-
-        @pl.when(jnp.logical_not(mine))
-        def _():
-            remote(osend.at[0], orecv.at[i], o_send.at[1], o_recv.at[i], kv, tp).wait_recv()
+        arrived(orecv.at[0:7], o_rsem)
 
     sums = []
     for q in range(2):
@@ -430,13 +385,20 @@
     bottom = jnp.where(lane16, pltpu.roll(sums[0], 64, axis=1), sums[1])
     out_ref[...] = jnp.concatenate([top, bottom], axis=0).astype(BF16)
 
-    for group in [acts_cp, d_cp, k_cp, e_cp, n_cp, o_cp, [cp for _, cp in p_cp]] + w_cp + a_cp + g_cp:
-        for cp in group:
-            cp.wait_send()
+    for ref, sem in (
+        (acts_t.at[0:128, :], acts_ssem), (acts_t.at[0:96, :], d_ssem), (wsend.at[0:7], w_ssem),
+        (kbuf.at[0:7], k_ssem), (qbuf.at[0:7], q_ssem), (wog.at[0:7], g_ssem), (arecv, a_ssem),
+        (frecv.at[:, 1:5], p_ssem), (frecv.at[:, 0, 0:7], h_ssem), (erecv.at[0:7], e_ssem), (nrm.at[0:7], n_ssem),
+    ):
+        sent(ref, sem)
 
     @pl.when(owner != tp)
     def _():
-        straight.wait_send()
+        sent(osend.at[0:8], o_ssem)
+
+    @pl.when(owner == tp)
+    def _():
+        sent(osend.at[0:7], o_ssem)
 
 
 def per_device(
@@ -478,16 +440,8 @@
         pltpu.VMEM((8, 2048), F32),
         pltpu.VMEM((2, 4, 256, 128), BF16),
         dma((len(operands),)),
-        dma((4,)), dma((4,)),
-        dma((3, 8)), dma((3, 8)),
-        dma((8,)), dma((8,)), dma((8,)), dma((8,)),
-        dma((3, 3)), dma((3, 3)),
-        dma((3, 5, 8)), dma((3, 5, 8)),
-        dma((8,)), dma((8,)),
-        dma((8,)), dma((8,)),
-        dma((2, 4)), dma((2, 4)),
-        dma((8,)), dma((8,)),
-        dma((4,)), dma((4,)),
+        dma, dma((4,)), dma, dma, dma, dma((3,)), dma, dma, dma, dma, dma, dma((4,)),
+        dma, dma((3,)), dma, dma((3,)), dma, dma((3,)), dma, dma, dma, dma, dma, dma,
         pltpu.SemaphoreType.REGULAR,
     ]
     operands = [pltpu.with_memory_space_constraint(x, pltpu.HBM) for x in operands]

time: 42 us -> 37.8 us (0.90)
  Pallas kernels: 39.7 us -> 35.5 us
    pallas_call x1, Pallas kernels: 39.7 us -> 35.5 us  [per_device(): pl.pallas_call(mixer_kernel, out_shape=(pltpu.VMEM((32, 128), BF16), pltp...]
where the time goes in v4:
time: 37.8 us; the launch traced here: 37.7 us
  Pallas kernels  35.5 us (94%)
  local copies, waits for them, and re-layouts  1.57 us (4%)
  between operations  0.65 us (2%)
    pallas_call x1, Pallas kernels, per_device(): pl.pallas_call(mixer_kernel, out_shape=(pltpu.VMEM((32, 128), BF16), pltp...  35.5 us
    unnamed x2, local copies, waits for them, and re-layouts  1.57 us

profile of v4, /device:TPU:1, one launch (start us, length us, event | category | flops | bytes accessed | tf_op | source)
XLA Modules:
  0.0 37.7 jit_solution(9124877417480798386)
XLA Ops:
  0.6 35.5 %mixer.1 = (bf16[32,128]{1,0:T(8,128)(2,1)S(1)}, f32[2,4,256,128]{3,2,1,0:T(8,128)S(1)}) custom-call(s32[2]{0:T(128)} %acc.1, bf16[32,512]{1,0:T(8,128)(2,1)} %bitcast.18, f32[1,32]{1,0:T(1,128)} %bitcast.24, bf16[32,1024]{1,0:T(8,128)(2,1)} %wg.1, bf16[32,1024]{1,0:T(8,128)(2,1)} %wv.1, bf16[32,512]{1,0:T(8,128)(2,1)} %ww.1, bf16[32,512]{1,0:T(8,128)(2,1)} %wr.1, ...), custom_call_target="tpu_custom_call" | custom-call | flops 1000000000 | bytes 4000000 | tf_op jit(solution)/shard_map/mixer/pallas_call | solution.py:448
  36.1 0.6 %copy.26 = bf16[128,32]{0,1:T(8,128)(2,1)} copy(bf16[128,32]{0,1:T(8,128)(2,1)S(1)} %bitcast.15) | data formatting | bytes 16384
  36.7 1.0 %copy.27 = f32[2,16,64,128]{3,2,1,0:T(8,128)} copy(f32[2,16,64,128]{3,2,1,0:T(8,128)S(1)} %bitcast.14) | data formatting | bytes 2097152

commit v5 on v4

--- a/solution.py
+++ b/solution.py
@@ -25,10 +25,10 @@
     out_ref, st_out,
     acc_s, hid_v, gain_v, wg_v, wv_v, ww_v, wr_v, ws_v, rawv_v, raww_v, rawr_v, tv_v, tw_v, tr_v, bias_v, rate_v, dgain_v,
     ppre_v, extra_v, ngain_v, wo_v,
-    acts_t, wsend, wblk, kbuf, qbuf, acts_f, acts_b, psend, arecv, bsend, frecv, esend, erecv, nrm, wog, osend, orecv,
+    acts_t, wsend, wblk, kbuf, qbuf, acts_f, acts_b, psend, arecv, bsend, frecv, esend, erecv, efar, nrm, wog, osend, orecv,
     base, state_b,
     lsem, acts_ssem, acts_rsem, d_ssem, d_rsem, w_ssem, w_rsem, k_ssem, k_rsem, q_ssem, q_rsem, g_ssem, g_rsem,
-    a_ssem, a_rsem, p_ssem, p_rsem, h_ssem, h_rsem, e_ssem, e_rsem, n_ssem, n_rsem, o_ssem, o_rsem, ready,
+    a_ssem, a_rsem, p_ssem, p_rsem, h_ssem, h_rsem, e_ssem, e_rsem, x_ssem, x_rsem, n_ssem, n_rsem, o_ssem, o_rsem, ready,
 ):
     kv = lax.axis_index("kv")
     tp = lax.axis_index("tp")
@@ -56,7 +56,7 @@
     barrier = pltpu.get_barrier_semaphore()
     for r in range(1, 8):
         pl.semaphore_signal(barrier, inc=1, device_id={"kv": plane(r), "tp": tp}, device_id_type=MESH)
-    for r in range(1, 8):
+    for r in (1, 7):
         pl.semaphore_signal(barrier, inc=1, device_id={"kv": ring(r), "tp": tp}, device_id_type=MESH)
     for r in range(1, 4):
         pl.semaphore_signal(barrier, inc=1, device_id={"kv": kv, "tp": lax.rem(tp + r, 4)}, device_id_type=MESH)
@@ -92,9 +92,7 @@
         wblk[t, own32, :] = wsend[c, t]
     kbuf[c] = jnp.concatenate([ws_v[...].astype(F32), jnp.zeros((16, 96), F32)], axis=1).astype(BF16)
 
-    pl.semaphore_wait(barrier, 17)
-    for r in range(1, 4):
-        pl.semaphore_signal(ready, inc=1, device_id={"kv": kv, "tp": lax.rem(tp + r, 4)}, device_id_type=MESH)
+    pl.semaphore_wait(barrier, 12)
 
     partner = z * 8 + c + 1 - 2 * lax.rem(c, 2)
 
@@ -226,16 +224,17 @@
             cc = lax.rem(c + r, 8)
             remote(src.at[cc], frecv.at[t, slot, c], ssem, rsem, lax.rem(z + dz, 8) * 8 + cc, tp).start()
 
+    def token_block(away):
+        return acts_b[pl.ds(pl.multiple_of(lax.rem(z + away, 8) * 64, 64), 64), :]
+
+    lhs = jnp.concatenate([token_block(away) for away in (4, 3, 5)], axis=0)
     for t in range(3):
         arrived(wblk.at[t, 0:224, :], w_rsem.at[t])
-        part = jnp.dot(acts_b[...], wblk[t], preferred_element_type=F32)
-        psend[t] = part.reshape(8, 8, 8, 128).astype(BF16)
-        for kind, away, to in ((2, 4, far * 8 + c), (0, 3, ring(1)), (1, 5, ring(7))):
-            remote(psend.at[t, lax.rem(z + away, 8)], arecv.at[t, kind], a_ssem, a_rsem.at[t], to, tp).start()
-        to_owners(psend.at[t, lax.rem(z + 1, 8)], t, 1, 1, p_ssem, p_rsem.at[t])
-        to_owners(psend.at[t, lax.rem(z + 7, 8)], t, 2, 7, p_ssem, p_rsem.at[t])
-        to_owners(psend.at[t, z], t, 0, 0, h_ssem, h_rsem.at[t])
-        frecv[t, 0, c] = psend[t, z, c]
+        part = jnp.dot(lhs, wblk[t], preferred_element_type=F32)
+        for i, (kind, away, to) in enumerate(((2, 4, far * 8 + c), (0, 3, ring(1)), (1, 5, ring(7)))):
+            zz = lax.rem(z + away, 8)
+            psend[t, zz] = part[i * 64:i * 64 + 64, :].reshape(8, 8, 128).astype(BF16)
+            remote(psend.at[t, zz], arecv.at[t, kind], a_ssem, a_rsem.at[t], to, tp).start()
     arrived(kbuf.at[0:7], k_rsem)
     arrived(qbuf.at[0:7], q_rsem)
     own_rows = jnp.concatenate(
@@ -256,9 +255,19 @@
         lower = jnp.where(low_half, pltpu.roll(jnp.where(low_half, rest, 0.0), 16, axis=1), rest)
         esend[k] = jnp.where(low_half, high + lower, jnp.where(row8 < 4, high, lower)).astype(BF16)
     erecv[z] = esend[z]
-    for r in (4, 3, 5, 2, 6, 1, 7):
+    remote(esend.at[lax.rem(z + 4, 8)], efar, e_ssem, x_rsem, far * 8 + c, tp).start()
+    lhs = jnp.concatenate([token_block(away) for away in (1, 7, 0, 2, 6)], axis=0)
+    for t in range(3):
+        part = jnp.dot(lhs, wblk[t], preferred_element_type=F32)
+        for i, away in enumerate((1, 7, 0, 2, 6)):
+            psend[t, lax.rem(z + away, 8)] = part[i * 64:i * 64 + 64, :].reshape(8, 8, 128).astype(BF16)
+        to_owners(psend.at[t, lax.rem(z + 1, 8)], t, 1, 1, p_ssem, p_rsem.at[t])
+        to_owners(psend.at[t, lax.rem(z + 7, 8)], t, 2, 7, p_ssem, p_rsem.at[t])
+        to_owners(psend.at[t, z], t, 0, 0, h_ssem, h_rsem.at[t])
+        frecv[t, 0, c] = psend[t, z, c]
+    arrived(wog.at[0:2], g_rsem.at[1])
+    for r in (3, 5, 2, 6, 1, 7):
         remote(esend.at[lax.rem(z + r, 8)], erecv.at[z], e_ssem, e_rsem, ring(r), tp).start()
-    arrived(wog.at[0:2], g_rsem.at[1])
     for t in range(3):
         arrived(arecv.at[t], a_rsem.at[t])
         extra_block = arecv[t, 2].astype(F32)
@@ -269,6 +278,9 @@
         bsend[t, 1] = (minus + jnp.where(even, zero_block, extra_block)).astype(BF16)
         to_owners(bsend.at[t, 0], t, 3, 2, p_ssem, p_rsem.at[t])
         to_owners(bsend.at[t, 1], t, 4, 6, p_ssem, p_rsem.at[t])
+    arrived(efar, x_rsem)
+    back = lax.rem(z + 6 + 4 * lax.rem(z, 2), 8)
+    remote(efar, erecv.at[back], x_ssem, e_rsem, far * 8 + c, tp).start()
     pass_on(2)
 
     arrived(erecv.at[0:7], e_rsem)
@@ -343,6 +355,8 @@
     for r in (4, 3, 5, 2, 6, 1, 7):
         remote(nrm.at[c], nrm.at[c], n_ssem, n_rsem, plane(r), tp).start()
     arrived(wog.at[0:2], g_rsem.at[2])
+    for r in range(1, 4):
+        pl.semaphore_signal(ready, inc=1, device_id={"kv": kv, "tp": lax.rem(tp + r, 4)}, device_id_type=MESH)
     pass_on(3)
     arrived(wog.at[0], g_rsem.at[3])
     pl.semaphore_wait(ready, 3)
@@ -388,7 +402,8 @@
     for ref, sem in (
         (acts_t.at[0:128, :], acts_ssem), (acts_t.at[0:96, :], d_ssem), (wsend.at[0:7], w_ssem),
         (kbuf.at[0:7], k_ssem), (qbuf.at[0:7], q_ssem), (wog.at[0:7], g_ssem), (arecv, a_ssem),
-        (frecv.at[:, 1:5], p_ssem), (frecv.at[:, 0, 0:7], h_ssem), (erecv.at[0:7], e_ssem), (nrm.at[0:7], n_ssem),
+        (frecv.at[:, 1:5], p_ssem), (frecv.at[:, 0, 0:7], h_ssem), (erecv.at[0:7], e_ssem), (efar, x_ssem),
+        (nrm.at[0:7], n_ssem),
     ):
         sent(ref, sem)
 
@@ -399,6 +414,14 @@
     @pl.when(owner == tp)
     def _():
         sent(osend.at[0:7], o_ssem)
+
+
+def hand_out(a, b, a_out, b_out, sem):
+    copies = [pltpu.make_async_copy(b, b_out, sem.at[0]), pltpu.make_async_copy(a, a_out, sem.at[1])]
+    for cp in copies:
+        cp.start()
+    for cp in copies:
+        cp.wait()
 
 
 def per_device(
@@ -433,6 +456,7 @@
         pltpu.VMEM((3, 5, 8, 8, 128), BF16),
         pltpu.VMEM((8, 8, 128), BF16),
         pltpu.VMEM((8, 8, 128), BF16),
+        pltpu.VMEM((8, 128), BF16),
         pltpu.VMEM((8, 16, 512), BF16),
         pltpu.VMEM((8, 32, 1024), BF16),
         pltpu.VMEM((8, 16, 128), BF16),
@@ -441,7 +465,7 @@
         pltpu.VMEM((2, 4, 256, 128), BF16),
         dma((len(operands),)),
         dma, dma((4,)), dma, dma, dma, dma((3,)), dma, dma, dma, dma, dma, dma((4,)),
-        dma, dma((3,)), dma, dma((3,)), dma, dma((3,)), dma, dma, dma, dma, dma, dma,
+        dma, dma((3,)), dma, dma((3,)), dma, dma((3,)), dma, dma, dma, dma, dma, dma, dma, dma,
         pltpu.SemaphoreType.REGULAR,
     ]
     operands = [pltpu.with_memory_space_constraint(x, pltpu.HBM) for x in operands]
@@ -460,6 +484,19 @@
         cost_estimate=pl.CostEstimate(flops=10**9, bytes_accessed=4 * 10**6, transcendentals=10**5),
         name="mixer",
     )(*operands)
+    out, state = [pltpu.with_memory_space_constraint(x, pltpu.VMEM) for x in (out, state)]
+    out, state = pl.pallas_call(
+        hand_out,
+        out_shape=(
+            jax.ShapeDtypeStruct((32, 128), BF16),
+            jax.ShapeDtypeStruct((2, 4, 256, 128), F32),
+        ),
+        in_specs=[pl.BlockSpec(memory_space=pltpu.VMEM)] * 2,
+        out_specs=(pl.BlockSpec(memory_space=pl.ANY),) * 2,
+        scratch_shapes=[pltpu.SemaphoreType.DMA((2,))],
+        compiler_params=pltpu.CompilerParams(vmem_limit_bytes=32 * 1024 * 1024),
+        name="hand_out",
+    )(out, state)
     return out.T, state.reshape(2, 16, 64, 128)
 
 

time: 37.8 us -> 35.8 us (0.947); the launches traced: 37.7 us -> 35.1 us
  local copies, waits for them, and re-layouts: 1.57 us -> 0 us
  Pallas kernels: 35.5 us -> 34.4 us
    pallas_call x1, Pallas kernels: 35.5 us -> 33.5 us  [per_device(): pl.pallas_call(mixer_kernel, out_shape=(pltpu.VMEM((32, 128), BF16), pltp...]
    unnamed x2 -> x0, local copies, waits for them, and re-layouts: 1.57 us -> none
    pallas_call x0 -> x1, Pallas kernels: none -> 0.99 us  [per_device(): pl.pallas_call(hand_out, out_shape=(jax.ShapeDtypeStruct((32, 128), BF16)...]
where the time goes in v5:
time: 35.8 us; the launch traced here: 35.1 us
  Pallas kernels  34.4 us (96%)
  between operations  0.65 us (2%)
    pallas_call x1, Pallas kernels, per_device(): pl.pallas_call(mixer_kernel, out_shape=(pltpu.VMEM((32, 128), BF16), pltp...  33.5 us
    pallas_call x1, Pallas kernels, per_device(): pl.pallas_call(hand_out, out_shape=(jax.ShapeDtypeStruct((32, 128), BF16)...  0.99 us

profile of v5, /device:TPU:1, one launch (start us, length us, event | category | flops | bytes accessed | tf_op | source)
XLA Modules:
  0.0 35.1 jit_solution(11037548657412013138)
XLA Ops:
  0.6 33.5 %mixer.1 = (bf16[32,128]{1,0:T(8,128)(2,1)S(1)}, f32[2,4,256,128]{3,2,1,0:T(8,128)S(1)}) custom-call(s32[2]{0:T(128)} %acc.1, bf16[32,512]{1,0:T(8,128)(2,1)} %bitcast.17, f32[1,32]{1,0:T(1,128)} %bitcast.24, bf16[32,1024]{1,0:T(8,128)(2,1)} %wg.1, bf16[32,1024]{1,0:T(8,128)(2,1)} %wv.1, bf16[32,512]{1,0:T(8,128)(2,1)} %ww.1, bf16[32,512]{1,0:T(8,128)(2,1)} %wr.1, ...), custom_call_target="tpu_custom_call" | custom-call | flops 1000000000 | bytes 4000000 | tf_op jit(solution)/shard_map/mixer/pallas_call | solution.py:472
  34.1 1.0 %hand_out.1 = (bf16[32,128]{1,0:T(8,128)(2,1)}, f32[2,4,256,128]{3,2,1,0:T(8,128)}) custom-call(bf16[32,128]{1,0:T(8,128)(2,1)S(1)} %get-tuple-element.6.a, f32[2,4,256,128]{3,2,1,0:T(8,128)S(1)} %get-tuple-element.7.b), custom_call_target="tpu_custom_call" | custom-call | tf_op jit(solution)/shard_map/hand_out/pallas_call | solution.py:488

commit v6 on v5

--- a/solution.py
+++ b/solution.py
@@ -9,7 +9,6 @@
 F32 = jnp.float32
 BF16 = jnp.bfloat16
 EPS = 1e-6
-PRIOR = 19
 
 
 def silu(x):
@@ -23,12 +22,11 @@
 def mixer_kernel(
     acc, hid, gain, wg, wv, ww, wr, ws, rawv, raww, rawr, tv, tw, tr, bias, rate, dgain, ppre, extra, prior, ngain, wo,
     out_ref, st_out,
-    acc_s, hid_v, gain_v, wg_v, wv_v, ww_v, wr_v, ws_v, rawv_v, raww_v, rawr_v, tv_v, tw_v, tr_v, bias_v, rate_v, dgain_v,
-    ppre_v, extra_v, ngain_v, wo_v,
+    acc_s, hid_v, gain_v, wide_v, narrow_v, ws_v, wo_v, rawv_v, raw_v, tv_v, tap_v, head_v, ppre_v, extra_v, ngain_v,
     acts_t, wsend, wblk, kbuf, qbuf, acts_f, acts_b, psend, arecv, bsend, frecv, esend, erecv, efar, nrm, wog, osend, orecv,
     base, state_b,
-    lsem, acts_ssem, acts_rsem, d_ssem, d_rsem, w_ssem, w_rsem, k_ssem, k_rsem, q_ssem, q_rsem, g_ssem, g_rsem,
-    a_ssem, a_rsem, p_ssem, p_rsem, h_ssem, h_rsem, e_ssem, e_rsem, x_ssem, x_rsem, n_ssem, n_rsem, o_ssem, o_rsem, ready,
+    lsem, acts_rsem, d_rsem, w_rsem, k_rsem, q_rsem, g_rsem, a_rsem, p_rsem, h_rsem, e_rsem, x_rsem, n_rsem, o_rsem,
+    ready,
 ):
     kv = lax.axis_index("kv")
     tp = lax.axis_index("tp")
@@ -47,11 +45,15 @@
             device_id={"kv": kv_to, "tp": tp_to}, device_id_type=MESH,
         )
 
+    acts_ssem, d_ssem, w_ssem, k_ssem, q_ssem, g_ssem, a_ssem, p_ssem, h_ssem, e_ssem, x_ssem, n_ssem, o_ssem = [
+        lsem.at[i] for i in (0, 1, 2, 3, 4, 5, 6, 7, 8, 9, 10, 11, 12)
+    ]
+
     def arrived(ref, sem):
         remote(ref, ref, acts_ssem, sem, kv, tp).wait_recv()
 
     def sent(ref, sem):
-        remote(ref, ref, sem, d_rsem, kv, tp).wait_send()
+        remote(ref, ref, sem, e_rsem, kv, tp).wait_send()
 
     barrier = pltpu.get_barrier_semaphore()
     for r in range(1, 8):
@@ -62,26 +64,31 @@
         pl.semaphore_signal(barrier, inc=1, device_id={"kv": kv, "tp": lax.rem(tp + r, 4)}, device_id_type=MESH)
 
     pairs = [
-        (acc, acc_s),
-        (hid, hid_v), (gain, gain_v), (wg, wg_v), (wv, wv_v), (ww, ww_v), (wr, wr_v), (ws, ws_v), (wo, wo_v),
-        (rawv, rawv_v), (raww, raww_v), (rawr, rawr_v), (tv, tv_v), (tw, tw_v), (tr, tr_v), (bias, bias_v),
-        (rate, rate_v), (dgain, dgain_v), (ppre, ppre_v), (extra, extra_v), (ngain, ngain_v), (prior, st_out),
+        ([hid], hid_v), ([gain], gain_v), ([wg, wv], wide_v), ([ww, wr], narrow_v), ([ws], ws_v), ([wo], wo_v),
+        ([acc], acc_s), ([rawv], rawv_v), ([raww, rawr], raw_v), ([tv], tv_v), ([tw, tr], tap_v),
+        ([bias, rate, dgain], head_v), ([ppre], ppre_v), ([extra], extra_v), ([ngain], ngain_v), ([prior], st_out),
     ]
-    loads = [pltpu.make_async_copy(s, d, lsem.at[i]) for i, (s, d) in enumerate(pairs)]
-    for cp in loads:
-        cp.start()
+    loads = []
+    for i, (sources, target) in enumerate(pairs):
+        for j, source in enumerate(sources):
+            pltpu.make_async_copy(source, target.at[j] if len(sources) > 1 else target, lsem.at[i]).start()
+        loads.append(pltpu.make_async_copy(target, target, lsem.at[i]))
 
     own32 = pl.ds(pl.multiple_of(c * 32, 32), 32)
+    loads[0].wait()
     loads[1].wait()
-    loads[2].wait()
     diag = lax.broadcasted_iota(jnp.int32, (32, 32), 0) == lax.broadcasted_iota(jnp.int32, (32, 32), 1)
     gcol = jnp.sum(jnp.where(diag, jnp.broadcast_to(gain_v[...], (32, 32)), 0.0), axis=1, keepdims=True)
     hidden = hid_v[...].astype(F32)
-    acts_t[own32, :] = (hidden * gcol).astype(BF16)
+    hidden = pltpu.roll(hidden, lax.rem(13 - z, 8) * 64, axis=1)
+    scaled = (hidden * gcol).astype(BF16)
+    for h in range(2):
+        acts_t[h, own32, :] = scaled[:, h * 256:(h + 1) * 256]
     squares = jnp.sum(hidden * hidden, axis=0, keepdims=True)
     qbuf[c] = jnp.concatenate([squares[:, i * 128:(i + 1) * 128] for i in range(4)], axis=0)
-    for i in range(3, 8):
+    for i in range(2, 5):
         loads[i].wait()
+    wg_v, wv_v, ww_v, wr_v = wide_v.at[0], wide_v.at[1], narrow_v.at[0], narrow_v.at[1]
     for j in range(8):
         lane = slice(j * 128, j * 128 + 128)
         half = slice((j % 4) * 128, (j % 4) * 128 + 128)
@@ -99,31 +106,53 @@
     def same_core(i):
         return pl.ds(pl.multiple_of(lax.rem(c + 8 - 2 * i, 8) * 32, 32), 32)
 
-    for i in (2, 1, 3):
-        remote(acts_t.at[own32, :], acts_t.at[own32, :], acts_ssem, acts_rsem.at[i], plane(2 * i), tp).start()
-    remote(acts_t.at[own32, :], acts_t.at[own32, :], acts_ssem, d_rsem, partner, tp).start()
-    for t in range(3):
+    def send_hidden(h):
+        own = acts_t.at[h, own32, :]
+        for i in (2, 1, 3):
+            remote(own, own, acts_ssem, acts_rsem.at[h, i - 1], plane(2 * i), tp).start()
+        remote(own, own, acts_ssem, d_rsem.at[h], partner, tp).start()
+
+    def send_weights(t):
         for r in (4, 3, 5, 2, 6, 1, 7):
             remote(wsend.at[lax.rem(c + r, 8), t], wblk.at[t, own32, :], w_ssem, w_rsem.at[t], plane(r), tp).start()
-        if t == 0:
-            for r in (4, 3, 5, 2, 6, 1, 7):
-                remote(kbuf.at[c], kbuf.at[c], k_ssem, k_rsem, plane(r), tp).start()
-                remote(qbuf.at[c], qbuf.at[c], q_ssem, q_rsem, plane(r), tp).start()
-
-    loads[8].wait()
+
+    def hand_over(h):
+        for i in (1, 3, 2):
+            arrived(acts_t.at[h, own32, :], acts_rsem.at[h, i - 1])
+            block = acts_t.at[h, same_core(i), :]
+            remote(block, block, d_ssem, d_rsem.at[h], partner, tp).start()
+
+    def turn(h):
+        arrived(acts_t.at[h, 0:128, :], d_rsem.at[h])
+        for i in range(2):
+            block = jnp.transpose(acts_t[h, :, i * 128:(i + 1) * 128].astype(F32))
+            rows = slice(h * 256 + i * 128, h * 256 + i * 128 + 128)
+            acts_f[rows, :] = block
+            acts_b[rows, :] = block.astype(BF16)
+
+    send_hidden(0)
+    send_weights(0)
+    send_weights(1)
+    send_weights(2)
+    send_hidden(1)
+    for r in (4, 3, 5, 2, 6, 1, 7):
+        remote(kbuf.at[c], kbuf.at[c], k_ssem, k_rsem, plane(r), tp).start()
+        remote(qbuf.at[c], qbuf.at[c], q_ssem, q_rsem, plane(r), tp).start()
+
+    loads[5].wait()
     wog[z] = wo_v[...]
 
     def pass_on(hop):
         for way, step in ((0, 1), (1, 7)):
-            if hop == 3 and way == 1:
-                continue
             at = lax.rem(z + 8 * hop - step * hop, 8)
             remote(wog.at[at], wog.at[at], g_ssem, g_rsem.at[hop], ring(step), tp).start()
 
     pass_on(0)
 
-    for cp in loads[:1] + loads[9:]:
+    for cp in loads[6:]:
         cp.wait()
+    raww_v, rawr_v, tw_v, tr_v = raw_v.at[0], raw_v.at[1], tap_v.at[0], tap_v.at[1]
+    bias_v, rate_v, dgain_v = head_v.at[0], head_v.at[1], head_v.at[2]
     row8 = lax.broadcasted_iota(jnp.int32, (8, 1), 0)
     tok = lax.rem(row8, 4)
 
@@ -205,16 +234,10 @@
                 st_out[s, g, rows, :] = new
                 state_b[s, g, rows, :] = new.astype(BF16)
 
-    for i in (1, 3, 2):
-        arrived(acts_t.at[own32, :], acts_rsem.at[i])
-        remote(acts_t.at[same_core(i), :], acts_t.at[same_core(i), :], d_ssem, d_rsem, partner, tp).start()
+    hand_over(0)
     arrived(wog.at[0:2], g_rsem.at[0])
     pass_on(1)
-    arrived(acts_t.at[0:128, :], d_rsem)
-    for i in range(4):
-        block = jnp.transpose(acts_t[:, i * 128:(i + 1) * 128].astype(F32))
-        acts_f[i * 128:(i + 1) * 128, :] = block
-        acts_b[i * 128:(i + 1) * 128, :] = block.astype(BF16)
+    turn(0)
     turned = (((1,), (1,)), ((), ()))
     even = lax.rem(z, 2) == 0
     far = lax.rem(z + 2 + 4 * lax.rem(z, 2), 8)
@@ -224,17 +247,16 @@
             cc = lax.rem(c + r, 8)
             remote(src.at[cc], frecv.at[t, slot, c], ssem, rsem, lax.rem(z + dz, 8) * 8 + cc, tp).start()
 
-    def token_block(away):
-        return acts_b[pl.ds(pl.multiple_of(lax.rem(z + away, 8) * 64, 64), 64), :]
-
-    lhs = jnp.concatenate([token_block(away) for away in (4, 3, 5)], axis=0)
+    lhs = acts_b[0:192, :]
     for t in range(3):
         arrived(wblk.at[t, 0:224, :], w_rsem.at[t])
         part = jnp.dot(lhs, wblk[t], preferred_element_type=F32)
-        for i, (kind, away, to) in enumerate(((2, 4, far * 8 + c), (0, 3, ring(1)), (1, 5, ring(7)))):
+        for i, (kind, away, to) in enumerate(((0, 3, ring(1)), (2, 4, far * 8 + c), (1, 5, ring(7)))):
             zz = lax.rem(z + away, 8)
             psend[t, zz] = part[i * 64:i * 64 + 64, :].reshape(8, 8, 128).astype(BF16)
             remote(psend.at[t, zz], arecv.at[t, kind], a_ssem, a_rsem.at[t], to, tp).start()
+    hand_over(1)
+    turn(1)
     arrived(kbuf.at[0:7], k_rsem)
     arrived(qbuf.at[0:7], q_rsem)
     own_rows = jnp.concatenate(
@@ -253,13 +275,13 @@
         high = mixture.astype(BF16).astype(F32)
         rest = (mixture - high).astype(BF16).astype(F32)
         lower = jnp.where(low_half, pltpu.roll(jnp.where(low_half, rest, 0.0), 16, axis=1), rest)
-        esend[k] = jnp.where(low_half, high + lower, jnp.where(row8 < 4, high, lower)).astype(BF16)
+        esend[lax.rem(z + 3 + k, 8)] = jnp.where(low_half, high + lower, jnp.where(row8 < 4, high, lower)).astype(BF16)
     erecv[z] = esend[z]
     remote(esend.at[lax.rem(z + 4, 8)], efar, e_ssem, x_rsem, far * 8 + c, tp).start()
-    lhs = jnp.concatenate([token_block(away) for away in (1, 7, 0, 2, 6)], axis=0)
+    lhs = acts_b[192:512, :]
     for t in range(3):
         part = jnp.dot(lhs, wblk[t], preferred_element_type=F32)
-        for i, away in enumerate((1, 7, 0, 2, 6)):
+        for i, away in enumerate((6, 7, 0, 1, 2)):
             psend[t, lax.rem(z + away, 8)] = part[i * 64:i * 64 + 64, :].reshape(8, 8, 128).astype(BF16)
         to_owners(psend.at[t, lax.rem(z + 1, 8)], t, 1, 1, p_ssem, p_rsem.at[t])
         to_owners(psend.at[t, lax.rem(z + 7, 8)], t, 2, 7, p_ssem, p_rsem.at[t])
@@ -284,6 +306,7 @@
     pass_on(2)
 
     arrived(erecv.at[0:7], e_rsem)
+    remote(wog.at[back], wog.at[back], g_ssem, g_rsem.at[3], far * 8 + c, tp).start()
     esum = erecv[0].astype(F32)
     for k in range(1, 8):
         esum = esum + erecv[k].astype(F32)
@@ -357,7 +380,6 @@
     arrived(wog.at[0:2], g_rsem.at[2])
     for r in range(1, 4):
         pl.semaphore_signal(ready, inc=1, device_id={"kv": kv, "tp": lax.rem(tp + r, 4)}, device_id_type=MESH)
-    pass_on(3)
     arrived(wog.at[0], g_rsem.at[3])
     pl.semaphore_wait(ready, 3)
     arrived(nrm.at[0:7], n_rsem)
@@ -400,7 +422,7 @@
     out_ref[...] = jnp.concatenate([top, bottom], axis=0).astype(BF16)
 
     for ref, sem in (
-        (acts_t.at[0:128, :], acts_ssem), (acts_t.at[0:96, :], d_ssem), (wsend.at[0:7], w_ssem),
+        (acts_t.at[:, 0:128, :], acts_ssem), (acts_t.at[:, 0:96, :], d_ssem), (wsend.at[0:7], w_ssem),
         (kbuf.at[0:7], k_ssem), (qbuf.at[0:7], q_ssem), (wog.at[0:7], g_ssem), (arecv, a_ssem),
         (frecv.at[:, 1:5], p_ssem), (frecv.at[:, 0, 0:7], h_ssem), (erecv.at[0:7], e_ssem), (efar, x_ssem),
         (nrm.at[0:7], n_ssem),
@@ -417,7 +439,9 @@
 
 
 def hand_out(a, b, a_out, b_out, sem):
-    copies = [pltpu.make_async_copy(b, b_out, sem.at[0]), pltpu.make_async_copy(a, a_out, sem.at[1])]
+    copies = [pltpu.make_async_copy(b.at[s, pl.ds(g, 2)], b_out.at[s, pl.ds(g, 2)], sem.at[2 * s + g // 2])
+              for s in range(2) for g in (0, 2)]
+    copies.append(pltpu.make_async_copy(a, a_out, sem.at[4]))
     for cp in copies:
         cp.start()
     for cp in copies:
@@ -438,12 +462,26 @@
         direct_path_gain.reshape(1, 16), prior_step_preact, extra_log_decay, prior_state.reshape(2, 4, 256, 128),
         group_norm_gain.reshape(1, 1024), output_matrix.T,
     ]
-    buffers = [pltpu.SMEM((2,), jnp.int32)] + [
-        pltpu.VMEM(x.shape, x.dtype) for i, x in enumerate(operands) if i not in (0, PRIOR)
+    buffers = [
+        pltpu.SMEM((2,), jnp.int32),
+        pltpu.VMEM((32, 512), BF16),
+        pltpu.VMEM((1, 32), F32),
+        pltpu.VMEM((2, 32, 1024), BF16),
+        pltpu.VMEM((2, 32, 512), BF16),
+        pltpu.VMEM((16, 32), BF16),
+        pltpu.VMEM((32, 1024), BF16),
+        pltpu.VMEM((7, 2, 1024), BF16),
+        pltpu.VMEM((2, 7, 2, 512), BF16),
+        pltpu.VMEM((4, 1024), BF16),
+        pltpu.VMEM((2, 4, 512), BF16),
+        pltpu.VMEM((3, 1, 16), F32),
+        pltpu.VMEM((2, 4, 16), F32),
+        pltpu.VMEM((2, 8, 16), F32),
+        pltpu.VMEM((1, 1024), F32),
     ]
     dma = pltpu.SemaphoreType.DMA
     scratch = buffers + [
-        pltpu.VMEM((256, 512), BF16),
+        pltpu.VMEM((2, 256, 256), BF16),
         pltpu.VMEM((8, 3, 32, 128), BF16),
         pltpu.VMEM((3, 256, 128), BF16),
         pltpu.VMEM((8, 16, 128), BF16),
@@ -463,9 +501,8 @@
         pltpu.VMEM((8, 16, 128), BF16),
         pltpu.VMEM((8, 2048), F32),
         pltpu.VMEM((2, 4, 256, 128), BF16),
-        dma((len(operands),)),
-        dma, dma((4,)), dma, dma, dma, dma((3,)), dma, dma, dma, dma, dma, dma((4,)),
-        dma, dma((3,)), dma, dma((3,)), dma, dma((3,)), dma, dma, dma, dma, dma, dma, dma, dma,
+        dma((16,)),
+        dma((2, 3)), dma((2,)), dma((3,)), dma, dma, dma((4,)), dma((3,)), dma((3,)), dma((3,)), dma, dma, dma, dma,
         pltpu.SemaphoreType.REGULAR,
     ]
     operands = [pltpu.with_memory_space_constraint(x, pltpu.HBM) for x in operands]
@@ -493,7 +530,7 @@
         ),
         in_specs=[pl.BlockSpec(memory_space=pltpu.VMEM)] * 2,
         out_specs=(pl.BlockSpec(memory_space=pl.ANY),) * 2,
-        scratch_shapes=[pltpu.SemaphoreType.DMA((2,))],
+        scratch_shapes=[pltpu.SemaphoreType.DMA((5,))],
         compiler_params=pltpu.CompilerParams(vmem_limit_bytes=32 * 1024 * 1024),
         name="hand_out",
     )(out, state)

time: 35.8 us -> 35.2 us (0.983); the launches traced: 35.1 us -> 35.1 us
  no operation moved by 1% of the time
where the time goes in v6:
time: 35.2 us; the launch traced here: 35.1 us
  Pallas kernels  34.5 us (98%)
  between operations  0.65 us (2%)
    pallas_call x1, Pallas kernels, per_device(): pl.pallas_call(mixer_kernel, out_shape=(pltpu.VMEM((32, 128), BF16), pltp...  33.5 us
    pallas_call x1, Pallas kernels, per_device(): pl.pallas_call(hand_out, out_shape=(jax.ShapeDtypeStruct((32, 128), BF16)...  1.01 us

profile of v6, /device:TPU:1, one launch (start us, length us, event | category | flops | bytes accessed | tf_op | source)
XLA Modules:
  0.0 35.1 jit_solution(9899201054001109589)
XLA Ops:
  0.6 33.5 %mixer.1 = (bf16[32,128]{1,0:T(8,128)(2,1)S(1)}, f32[2,4,256,128]{3,2,1,0:T(8,128)S(1)}) custom-call(s32[2]{0:T(128)} %acc.1, bf16[32,512]{1,0:T(8,128)(2,1)} %bitcast.17, f32[1,32]{1,0:T(1,128)} %bitcast.24, bf16[32,1024]{1,0:T(8,128)(2,1)} %wg.1, bf16[32,1024]{1,0:T(8,128)(2,1)} %wv.1, bf16[32,512]{1,0:T(8,128)(2,1)} %ww.1, bf16[32,512]{1,0:T(8,128)(2,1)} %wr.1, ...), custom_call_target="tpu_custom_call" | custom-call | flops 1000000000 | bytes 4000000 | tf_op jit(solution)/shard_map/mixer/pallas_call | solution.py:509
  34.1 1.0 %hand_out.1 = (bf16[32,128]{1,0:T(8,128)(2,1)}, f32[2,4,256,128]{3,2,1,0:T(8,128)}) custom-call(bf16[32,128]{1,0:T(8,128)(2,1)S(1)} %get-tuple-element.6.a, f32[2,4,256,128]{3,2,1,0:T(8,128)S(1)} %get-tuple-element.7.b), custom_call_target="tpu_custom_call" | custom-call | tf_op jit(solution)/shard_map/hand_out/pallas_call | solution.py:525

commit v7 on v6

--- a/solution.py
+++ b/solution.py
@@ -16,7 +16,7 @@
 
 
 def softplus(x):
-    return jnp.maximum(x, 0.0) + jnp.log(1.0 + jnp.exp(-jnp.abs(x)))
+    return jnp.maximum(x, 0.0) + jnp.log1p(jnp.exp(-jnp.abs(x)))
 
 
 def mixer_kernel(
@@ -25,7 +25,7 @@
     acc_s, hid_v, gain_v, wide_v, narrow_v, ws_v, wo_v, rawv_v, raw_v, tv_v, tap_v, head_v, ppre_v, extra_v, ngain_v,
     acts_t, wsend, wblk, kbuf, qbuf, acts_f, acts_b, psend, arecv, bsend, frecv, esend, erecv, efar, nrm, wog, osend, orecv,
     base, state_b,
-    lsem, acts_rsem, d_rsem, w_rsem, k_rsem, q_rsem, g_rsem, a_rsem, p_rsem, h_rsem, e_rsem, x_rsem, n_rsem, o_rsem,
+    lsem, acts_rsem, d_rsem, w_rsem, k_rsem, q_rsem, g_rsem, a_rsem, p_rsem, h_rsem, b_rsem, e_rsem, x_rsem, n_rsem, o_rsem,
     ready,
 ):
     kv = lax.axis_index("kv")
@@ -45,8 +45,8 @@
             device_id={"kv": kv_to, "tp": tp_to}, device_id_type=MESH,
         )
 
-    acts_ssem, d_ssem, w_ssem, k_ssem, q_ssem, g_ssem, a_ssem, p_ssem, h_ssem, e_ssem, x_ssem, n_ssem, o_ssem = [
-        lsem.at[i] for i in (0, 1, 2, 3, 4, 5, 6, 7, 8, 9, 10, 11, 12)
+    acts_ssem, d_ssem, w_ssem, k_ssem, q_ssem, g_ssem, a_ssem, p_ssem, h_ssem, e_ssem, x_ssem, n_ssem, o_ssem, b_ssem = [
+        lsem.at[i] for i in range(14)
     ]
 
     def arrived(ref, sem):
@@ -90,14 +90,23 @@
         loads[i].wait()
     wg_v, wv_v, ww_v, wr_v = wide_v.at[0], wide_v.at[1], narrow_v.at[0], narrow_v.at[1]
     for j in range(8):
-        lane = slice(j * 128, j * 128 + 128)
-        half = slice((j % 4) * 128, (j % 4) * 128 + 128)
-        wsend[j, 0] = ww_v[:, half] if j < 4 else wr_v[:, half]
-        wsend[j, 1] = wv_v[:, lane]
-        wsend[j, 2] = wg_v[:, lane]
+        near = slice((j % 4) * 128, (j % 4) * 128 + 128)
+        wsend[j, 0] = (ww_v if j < 4 else wr_v)[:, near]
+        for h in range(2):
+            lane = slice((j % 4 + 4 * h) * 128, (j % 4 + 4 * h) * 128 + 128)
+            wsend[j, 1 + h] = (wv_v if j < 4 else wg_v)[:, lane]
     for t in range(3):
         wblk[t, own32, :] = wsend[c, t]
     kbuf[c] = jnp.concatenate([ws_v[...].astype(F32), jnp.zeros((16, 96), F32)], axis=1).astype(BF16)
+
+    loads[5].wait()
+    wog[z] = wo_v[...]
+
+    def pass_on(hop):
+        for way, step in ((0, 1), (1, 7)):
+            at = lax.rem(z + 8 * hop - step * hop, 8)
+            remote(wog.at[at], wog.at[at], g_ssem, g_rsem.at[hop], ring(step), tp).start()
+
 
     pl.semaphore_wait(barrier, 12)
 
@@ -132,22 +141,13 @@
 
     send_hidden(0)
     send_weights(0)
+    pass_on(0)
     send_weights(1)
     send_weights(2)
     send_hidden(1)
     for r in (4, 3, 5, 2, 6, 1, 7):
         remote(kbuf.at[c], kbuf.at[c], k_ssem, k_rsem, plane(r), tp).start()
         remote(qbuf.at[c], qbuf.at[c], q_ssem, q_rsem, plane(r), tp).start()
-
-    loads[5].wait()
-    wog[z] = wo_v[...]
-
-    def pass_on(hop):
-        for way, step in ((0, 1), (1, 7)):
-            at = lax.rem(z + 8 * hop - step * hop, 8)
-            remote(wog.at[at], wog.at[at], g_ssem, g_rsem.at[hop], ring(step), tp).start()
-
-    pass_on(0)
 
     for cp in loads[6:]:
         cp.wait()
@@ -283,10 +283,14 @@
         part = jnp.dot(lhs, wblk[t], preferred_element_type=F32)
         for i, away in enumerate((6, 7, 0, 1, 2)):
             psend[t, lax.rem(z + away, 8)] = part[i * 64:i * 64 + 64, :].reshape(8, 8, 128).astype(BF16)
-        to_owners(psend.at[t, lax.rem(z + 1, 8)], t, 1, 1, p_ssem, p_rsem.at[t])
-        to_owners(psend.at[t, lax.rem(z + 7, 8)], t, 2, 7, p_ssem, p_rsem.at[t])
-        to_owners(psend.at[t, z], t, 0, 0, h_ssem, h_rsem.at[t])
-        frecv[t, 0, c] = psend[t, z, c]
+    frecv[:, 0, c] = psend[:, z, c]
+    for slot, dz, rsem in ((1, 1, b_rsem), (2, 7, b_rsem), (0, 0, h_rsem)):
+        for r in range(0 if dz else 1, 8):
+            cc = lax.rem(c + r, 8)
+            zz = lax.rem(z + dz, 8)
+            remote(
+                psend.at[:, zz, cc], frecv.at[:, slot, c], b_ssem if dz else h_ssem, rsem, zz * 8 + cc, tp
+            ).start()
     arrived(wog.at[0:2], g_rsem.at[1])
     for r in (3, 5, 2, 6, 1, 7):
         remote(esend.at[lax.rem(z + r, 8)], erecv.at[z], e_ssem, e_rsem, ring(r), tp).start()
@@ -324,8 +328,10 @@
     ecum = jnp.exp(cum)
 
     def settle(t):
-        arrived(frecv.at[t, 1:5], p_rsem.at[t])
-        arrived(frecv.at[t, 0, 0:7], h_rsem.at[t])
+        if t == 0:
+            arrived(frecv.at[:, 1:3], b_rsem)
+            arrived(frecv.at[:, 0, 0:7], h_rsem)
+        arrived(frecv.at[t, 3:5], p_rsem.at[t])
 
     def fresh(t, j):
         x = frecv[t, 0, j].astype(F32)
@@ -353,42 +359,37 @@
         ]
         carried.append(jnp.where(row8 < 4, both[0], both[1]))
         inner.append([jnp.sum(reads[g] * down(writes[g], d), axis=1, keepdims=True) for d in range(4)])
-    settle(1)
-    mixed = []
-    for j in range(8):
-        g, i = j // 2, j % 2
-        value = conv(fresh(1, j), j * 128, tv_v, j * 128)
-        m = spread(ecum, j) * carried[g][:, i * 128:(i + 1) * 128] + spread(dg, j) * value
-        for d in range(4):
-            m = m + (inner[g][d] * spread(pair_w[d], j)) * down(value, d)
-        mixed.append(m)
-    settle(2)
-    normed = []
-    for g in range(4):
-        gated = [mixed[j] * silu(fresh(2, j)) for j in (2 * g, 2 * g + 1)]
-        mean = jnp.sum(gated[0] * gated[0] + gated[1] * gated[1], axis=1, keepdims=True) / 256.0
-        scale = lax.rsqrt(mean + EPS)
-        for i in range(2):
-            j = 2 * g + i
-            normed.append(gated[i] * scale * ngain_v[:, j * 128:(j + 1) * 128])
-    nrm[c] = jnp.concatenate(
-        [jnp.concatenate(normed[0:4], axis=1), jnp.concatenate(normed[4:8], axis=1)], axis=0
-    ).astype(BF16)
-
-    for r in (4, 3, 5, 2, 6, 1, 7):
-        remote(nrm.at[c], nrm.at[c], n_ssem, n_rsem, plane(r), tp).start()
+    for half in range(2):
+        settle(1 + half)
+        gated = []
+        for i in range(4):
+            j = 4 * half + i
+            g = j // 2
+            value = conv(fresh(1 + half, i), j * 128, tv_v, j * 128)
+            m = spread(ecum, j) * carried[g][:, (j % 2) * 128:(j % 2) * 128 + 128] + spread(dg, j) * value
+            for d in range(4):
+                m = m + (inner[g][d] * spread(pair_w[d], j)) * down(value, d)
+            gated.append(m * silu(fresh(1 + half, 4 + i)))
+        normed = []
+        for a, b in ((0, 1), (2, 3)):
+            mean = jnp.sum(gated[a] * gated[a] + gated[b] * gated[b], axis=1, keepdims=True) / 256.0
+            scale = lax.rsqrt(mean + EPS)
+            for i in (a, b):
+                j = 4 * half + i
+                normed.append(gated[i] * scale * ngain_v[:, j * 128:(j + 1) * 128])
+        nrm[half, c] = jnp.concatenate(normed, axis=1).astype(BF16)
+        for r in (4, 3, 5, 2, 6, 1, 7):
+            remote(nrm.at[half, c], nrm.at[half, c], n_ssem, n_rsem.at[half], plane(r), tp).start()
     arrived(wog.at[0:2], g_rsem.at[2])
     for r in range(1, 4):
         pl.semaphore_signal(ready, inc=1, device_id={"kv": kv, "tp": lax.rem(tp + r, 4)}, device_id_type=MESH)
     arrived(wog.at[0], g_rsem.at[3])
     pl.semaphore_wait(ready, 3)
-    arrived(nrm.at[0:7], n_rsem)
-
-    nall = nrm[...].astype(F32)
     wall = wog[...].reshape(256, 1024)
     p = None
     for i in range(2):
-        block = nall[:, i * 8:i * 8 + 8, :].reshape(64, 512).astype(BF16)
+        arrived(nrm.at[i, 0:7], n_rsem.at[i])
+        block = nrm[i].astype(F32).reshape(64, 512).astype(BF16)
         q = lax.dot_general(wall[:, i * 512:(i + 1) * 512], block, turned, preferred_element_type=F32)
         p = q if p is None else p + q
     for k in range(8):
@@ -424,8 +425,8 @@
     for ref, sem in (
         (acts_t.at[:, 0:128, :], acts_ssem), (acts_t.at[:, 0:96, :], d_ssem), (wsend.at[0:7], w_ssem),
         (kbuf.at[0:7], k_ssem), (qbuf.at[0:7], q_ssem), (wog.at[0:7], g_ssem), (arecv, a_ssem),
-        (frecv.at[:, 1:5], p_ssem), (frecv.at[:, 0, 0:7], h_ssem), (erecv.at[0:7], e_ssem), (efar, x_ssem),
-        (nrm.at[0:7], n_ssem),
+        (frecv.at[:, 3:5], p_ssem), (frecv.at[:, 0, 0:7], h_ssem), (frecv.at[:, 1:3], b_ssem), (erecv.at[0:7], e_ssem), (efar, x_ssem),
+        (nrm.at[:, 0:7], n_ssem),
     ):
         sent(ref, sem)
 
@@ -495,14 +496,14 @@
         pltpu.VMEM((8, 8, 128), BF16),
         pltpu.VMEM((8, 8, 128), BF16),
         pltpu.VMEM((8, 128), BF16),
-        pltpu.VMEM((8, 16, 512), BF16),
+        pltpu.VMEM((2, 8, 8, 512), BF16),
         pltpu.VMEM((8, 32, 1024), BF16),
         pltpu.VMEM((8, 16, 128), BF16),
         pltpu.VMEM((8, 16, 128), BF16),
         pltpu.VMEM((8, 2048), F32),
         pltpu.VMEM((2, 4, 256, 128), BF16),
         dma((16,)),
-        dma((2, 3)), dma((2,)), dma((3,)), dma, dma, dma((4,)), dma((3,)), dma((3,)), dma((3,)), dma, dma, dma, dma,
+        dma((2, 3)), dma((2,)), dma((3,)), dma, dma, dma((4,)), dma((3,)), dma((3,)), dma, dma, dma, dma, dma((2,)), dma,
         pltpu.SemaphoreType.REGULAR,
     ]
     operands = [pltpu.with_memory_space_constraint(x, pltpu.HBM) for x in operands]

time: 35.2 us -> 35.2 us (level)
  no operation moved by 1% of the time
where the time goes in v7:
time: 35.2 us; the launch traced here: 35.1 us
  Pallas kernels  34.5 us (98%)
  between operations  0.65 us (2%)
    pallas_call x1, Pallas kernels, per_device(): pl.pallas_call(mixer_kernel, out_shape=(pltpu.VMEM((32, 128), BF16), pltp...  33.5 us
    pallas_call x1, Pallas kernels, per_device(): pl.pallas_call(hand_out, out_shape=(jax.ShapeDtypeStruct((32, 128), BF16)...  1.01 us

profile of v7, /device:TPU:1, one launch (start us, length us, event | category | flops | bytes accessed | tf_op | source)
XLA Modules:
  0.0 35.1 jit_solution(8594458532989327549)
XLA Ops:
  0.6 33.5 %mixer.1 = (bf16[32,128]{1,0:T(8,128)(2,1)S(1)}, f32[2,4,256,128]{3,2,1,0:T(8,128)S(1)}) custom-call(s32[2]{0:T(128)} %acc.1, bf16[32,512]{1,0:T(8,128)(2,1)} %bitcast.17, f32[1,32]{1,0:T(1,128)} %bitcast.24, bf16[32,1024]{1,0:T(8,128)(2,1)} %wg.1, bf16[32,1024]{1,0:T(8,128)(2,1)} %wv.1, bf16[32,512]{1,0:T(8,128)(2,1)} %ww.1, bf16[32,512]{1,0:T(8,128)(2,1)} %wr.1, ...), custom_call_target="tpu_custom_call" | custom-call | flops 1000000000 | bytes 4000000 | tf_op jit(solution)/shard_map/mixer/pallas_call | solution.py:510
  34.1 1.0 %hand_out.1 = (bf16[32,128]{1,0:T(8,128)(2,1)}, f32[2,4,256,128]{3,2,1,0:T(8,128)}) custom-call(bf16[32,128]{1,0:T(8,128)(2,1)S(1)} %get-tuple-element.6.a, f32[2,4,256,128]{3,2,1,0:T(8,128)S(1)} %get-tuple-element.7.b), custom_call_target="tpu_custom_call" | custom-call | tf_op jit(solution)/shard_map/hand_out/pallas_call | solution.py:526

commit v8 on v7

--- a/solution.py
+++ b/solution.py
@@ -21,9 +21,9 @@
 
 def mixer_kernel(
     acc, hid, gain, wg, wv, ww, wr, ws, rawv, raww, rawr, tv, tw, tr, bias, rate, dgain, ppre, extra, prior, ngain, wo,
-    out_ref, st_out,
+    orecv, st_out,
     acc_s, hid_v, gain_v, wide_v, narrow_v, ws_v, wo_v, rawv_v, raw_v, tv_v, tap_v, head_v, ppre_v, extra_v, ngain_v,
-    acts_t, wsend, wblk, kbuf, qbuf, acts_f, acts_b, psend, arecv, bsend, frecv, esend, erecv, efar, nrm, wog, osend, orecv,
+    acts_t, wsend, wblk, kbuf, qbuf, acts_f, acts_b, psend, arecv, bsend, frecv, esend, erecv, efar, nrm, wog, osend,
     base, state_b,
     lsem, acts_rsem, d_rsem, w_rsem, k_rsem, q_rsem, g_rsem, a_rsem, p_rsem, h_rsem, b_rsem, e_rsem, x_rsem, n_rsem, o_rsem,
     ready,
@@ -251,7 +251,7 @@
     for t in range(3):
         arrived(wblk.at[t, 0:224, :], w_rsem.at[t])
         part = jnp.dot(lhs, wblk[t], preferred_element_type=F32)
-        for i, (kind, away, to) in enumerate(((0, 3, ring(1)), (2, 4, far * 8 + c), (1, 5, ring(7)))):
+        for i, (kind, away, to) in ((1, (2, 4, far * 8 + c)), (0, (0, 3, ring(1))), (2, (1, 5, ring(7)))):
             zz = lax.rem(z + away, 8)
             psend[t, zz] = part[i * 64:i * 64 + 64, :].reshape(8, 8, 128).astype(BF16)
             remote(psend.at[t, zz], arecv.at[t, kind], a_ssem, a_rsem.at[t], to, tp).start()
@@ -411,6 +411,28 @@
         orecv[slot] = osend[z]
         arrived(orecv.at[0:7], o_rsem)
 
+    for ref, sem in (
+        (acts_t.at[:, 0:128, :], acts_ssem), (acts_t.at[:, 0:96, :], d_ssem), (wsend.at[0:7], w_ssem),
+        (kbuf.at[0:7], k_ssem), (qbuf.at[0:7], q_ssem), (wog.at[0:7], g_ssem), (arecv, a_ssem),
+        (frecv.at[:, 3:5], p_ssem), (frecv.at[:, 0, 0:7], h_ssem), (frecv.at[:, 1:3], b_ssem), (erecv.at[0:7], e_ssem), (efar, x_ssem),
+        (nrm.at[:, 0:7], n_ssem),
+    ):
+        sent(ref, sem)
+
+    @pl.when(owner != tp)
+    def _():
+        sent(osend.at[0:8], o_ssem)
+
+    @pl.when(owner == tp)
+    def _():
+        sent(osend.at[0:7], o_ssem)
+
+
+def hand_out(orecv, b, a_out, b_out, out_v, sem):
+    copies = [pltpu.make_async_copy(b.at[s, pl.ds(g, 2)], b_out.at[s, pl.ds(g, 2)], sem.at[2 * s + g // 2])
+              for s in range(2) for g in (0, 2)]
+    for cp in copies:
+        cp.start()
     sums = []
     for q in range(2):
         s4 = orecv[q].astype(F32)
@@ -420,31 +442,9 @@
     lane16 = lax.broadcasted_iota(jnp.int32, (16, 128), 1) < 64
     top = jnp.where(lane16, sums[0], pltpu.roll(sums[1], 64, axis=1))
     bottom = jnp.where(lane16, pltpu.roll(sums[0], 64, axis=1), sums[1])
-    out_ref[...] = jnp.concatenate([top, bottom], axis=0).astype(BF16)
-
-    for ref, sem in (
-        (acts_t.at[:, 0:128, :], acts_ssem), (acts_t.at[:, 0:96, :], d_ssem), (wsend.at[0:7], w_ssem),
-        (kbuf.at[0:7], k_ssem), (qbuf.at[0:7], q_ssem), (wog.at[0:7], g_ssem), (arecv, a_ssem),
-        (frecv.at[:, 3:5], p_ssem), (frecv.at[:, 0, 0:7], h_ssem), (frecv.at[:, 1:3], b_ssem), (erecv.at[0:7], e_ssem), (efar, x_ssem),
-        (nrm.at[:, 0:7], n_ssem),
-    ):
-        sent(ref, sem)
-
-    @pl.when(owner != tp)
-    def _():
-        sent(osend.at[0:8], o_ssem)
-
-    @pl.when(owner == tp)
-    def _():
-        sent(osend.at[0:7], o_ssem)
-
-
-def hand_out(a, b, a_out, b_out, sem):
-    copies = [pltpu.make_async_copy(b.at[s, pl.ds(g, 2)], b_out.at[s, pl.ds(g, 2)], sem.at[2 * s + g // 2])
-              for s in range(2) for g in (0, 2)]
-    copies.append(pltpu.make_async_copy(a, a_out, sem.at[4]))
-    for cp in copies:
-        cp.start()
+    out_v[...] = jnp.concatenate([top, bottom], axis=0).astype(BF16)
+    copies.append(pltpu.make_async_copy(out_v, a_out, sem.at[4]))
+    copies[-1].start()
     for cp in copies:
         cp.wait()
 
@@ -499,7 +499,6 @@
         pltpu.VMEM((2, 8, 8, 512), BF16),
         pltpu.VMEM((8, 32, 1024), BF16),
         pltpu.VMEM((8, 16, 128), BF16),
-        pltpu.VMEM((8, 16, 128), BF16),
         pltpu.VMEM((8, 2048), F32),
         pltpu.VMEM((2, 4, 256, 128), BF16),
         dma((16,)),
@@ -510,7 +509,7 @@
     out, state = pl.pallas_call(
         mixer_kernel,
         out_shape=(
-            pltpu.VMEM((32, 128), BF16),
+            pltpu.VMEM((8, 16, 128), BF16),
             pltpu.VMEM((2, 4, 256, 128), F32),
         ),
         in_specs=[pl.BlockSpec(memory_space=pl.ANY)] * len(operands),
@@ -531,7 +530,7 @@
         ),
         in_specs=[pl.BlockSpec(memory_space=pltpu.VMEM)] * 2,
         out_specs=(pl.BlockSpec(memory_space=pl.ANY),) * 2,
-        scratch_shapes=[pltpu.SemaphoreType.DMA((5,))],
+        scratch_shapes=[pltpu.VMEM((32, 128), BF16), pltpu.SemaphoreType.DMA((5,))],
         compiler_params=pltpu.CompilerParams(vmem_limit_bytes=32 * 1024 * 1024),
         name="hand_out",
     )(out, state)

time: 35.2 us -> 35.2 us (level)
  no operation moved by 1% of the time
where the time goes in v8:
time: 35.2 us; the launch traced here: 35.1 us
  Pallas kernels  34.4 us (98%)
  between operations  0.65 us (2%)
    pallas_call x1, Pallas kernels, per_device(): pl.pallas_call(mixer_kernel, out_shape=(pltpu.VMEM((8, 16, 128), BF16), p...  33.4 us
    pallas_call x1, Pallas kernels, per_device(): pl.pallas_call(hand_out, out_shape=(jax.ShapeDtypeStruct((32, 128), BF16)...  1.01 us

profile of v8, /device:TPU:1, one launch (start us, length us, event | category | flops | bytes accessed | tf_op | source)
XLA Modules:
  0.0 35.1 jit_solution(4920223779607874900)
XLA Ops:
  0.6 33.4 %mixer.1 = (bf16[8,16,128]{2,1,0:T(8,128)(2,1)S(1)}, f32[2,4,256,128]{3,2,1,0:T(8,128)S(1)}) custom-call(s32[2]{0:T(128)} %acc.1, bf16[32,512]{1,0:T(8,128)(2,1)} %bitcast.17, f32[1,32]{1,0:T(1,128)} %bitcast.24, bf16[32,1024]{1,0:T(8,128)(2,1)} %wg.1, bf16[32,1024]{1,0:T(8,128)(2,1)} %wv.1, bf16[32,512]{1,0:T(8,128)(2,1)} %ww.1, bf16[32,512]{1,0:T(8,128)(2,1)} %wr.1, ...), custom_call_target="tpu_custom_call" | custom-call | flops 1000000000 | bytes 4000000 | tf_op jit(solution)/shard_map/mixer/pallas_call | solution.py:509
  34.1 1.0 %hand_out.1 = (bf16[32,128]{1,0:T(8,128)(2,1)}, f32[2,4,256,128]{3,2,1,0:T(8,128)}) custom-call(bf16[8,16,128]{2,1,0:T(8,128)(2,1)S(1)} %get-tuple-element.6.orecv, f32[2,4,256,128]{3,2,1,0:T(8,128)S(1)} %get-tuple-element.7.b), custom_call_target="tpu_custom_call" | custom-call | tf_op jit(solution)/shard_map/hand_out/pallas_call | solution.py:525
